TPU v7x, 256 devices: a 4x2x16 block of a 4x16x16 slice. The times are simulated.
256 devices in a mesh: grp: 2 (over y), fs: 16 (over z), tp: 8 (over x, core).
Axes of the slice: x: 4, y: 2, z: 16, core: 2. Of those that a mesh axis runs over, the one named last changes fastest.
The devices are a block of a 4x16x16 slice.
Arguments:
- stream: bfloat16 [2048, 12288], P('tp', ('grp', 'fs')), parts along dimension 1, may hold values from -6 to 6
- first_gain: float32 [2048], replicated, may hold values from 0.1 to 1.9
- first_gate: float32 [2048, 5632], P('fs', 'tp'), may hold values from -0.125 to 0.125
- first_gate_scale: float32 [5632], P('tp'), may hold values from 0.5 to 2
- first_up: float32 [2048, 5632], P('fs', 'tp'), may hold values from -0.125 to 0.125
- first_up_scale: float32 [5632], P('tp'), may hold values from 0.5 to 2
- first_down: float32 [5632, 2048], P('tp', 'fs'), may hold values from -0.078125 to 0.078125
- first_down_scale: float32 [2048], P('fs'), may hold values from 0.5 to 2
- mixer_gain: float32 [2048], replicated, may hold values from 0.1 to 1.9
- mixer_left: float32 [2048, 1024], P('fs', 'tp'), may hold values from -0.125 to 0.125
- mixer_left_scale: float32 [1024], P('tp'), may hold values from 0.5 to 2
- mixer_right: float32 [2048, 1024], P('fs', 'tp'), may hold values from -0.125 to 0.125
- mixer_right_scale: float32 [1024], P('tp'), may hold values from 0.5 to 2
- channel_gain: float32 [1024], P('tp'), may hold values from 0.1 to 1.9
- spatial: bfloat16 [8, 128, 128], P('tp'), may hold values from -0.5 to 0.5
- spatial_bias: float32 [8, 128], P('tp'), may hold values from 0.1 to 1.9
- mixer_out: float32 [1024, 2048], P('tp', 'fs'), may hold values from -0.1875 to 0.1875
- mixer_out_scale: float32 [2048], P('fs'), may hold values from 0.5 to 2
- second_gain: float32 [2048], replicated, may hold values from 0.1 to 1.9
- second_gate: float32 [2048, 5632], P('fs', 'tp'), may hold values from -0.125 to 0.125
- second_gate_scale: float32 [5632], P('tp'), may hold values from 0.5 to 2
- second_up: float32 [2048, 5632], P('fs', 'tp'), may hold values from -0.125 to 0.125
- second_up_scale: float32 [5632], P('tp'), may hold values from 0.5 to 2
- second_down: float32 [5632, 2048], P('tp', 'fs'), may hold values from -0.078125 to 0.078125
- second_down_scale: float32 [2048], P('fs'), may hold values from 0.5 to 2
Outputs:
- result: bfloat16 [2048, 12288], P('tp', ('grp', 'fs')), parts along dimension 1
There are 2 independent parts, one for each index of `grp`. A program takes and returns all parts, laid end to end along the dimension named above; an argument that names none is the same for every part. Nothing has to cross between parts.
All inputs are finite; a program needn't handle non-finite values.
Results may differ from a plain program's by a relative error of at most 0.02.
Values may be sent and summed in bfloat16 or wider, within the bound.
A program may use at most 128 MiB of HBM per device.

v0:
```python
import jax
import jax.numpy as jnp
from jax import lax
from jax.sharding import PartitionSpec as P

BRANCH = 1024


EPS = 1e-06


def laid_out(parts, dim):
    lengths = list(parts.shape[1:])
    lengths[dim] *= parts.shape[0]
    return jnp.moveaxis(parts, 0, dim).reshape(lengths)


def copy_for_each(value, axis):
    copies = jnp.broadcast_to(value, (lax.axis_size(axis), *value.shape))
    return lax.all_to_all(copies, axis, split_axis=0, concat_axis=0, tiled=True)


def gather_directly(value, axis, dim):
    return laid_out(copy_for_each(value, axis), dim)


def over_copies(value, axis):
    return copy_for_each(value, axis).sum(axis=0)


def in_one(arrays, axis):
    ravelled, at, outs = (jnp.concatenate([a.reshape(-1) for a in arrays]), 0, [])
    running = over_copies(ravelled, axis)
    for a in arrays:
        outs.append(running[at : at + a.size].reshape(a.shape))
        at += a.size
    return tuple(outs)


def cut_along(value, dim, peers):
    lengths = value.shape
    parts = value.reshape(*lengths[:dim], peers, lengths[dim] // peers, *lengths[dim + 1 :])
    return jnp.moveaxis(parts, dim, 0)


def summed_on_arrival(value, axis, dim):
    parts = cut_along(value, dim, lax.axis_size(axis))
    arrived = lax.all_to_all(parts, axis, split_axis=0, concat_axis=0, tiled=True)
    return arrived.astype(jnp.float32).sum(axis=0)


def turned_gather(arrays, axis, dims):
    turned = [jnp.moveaxis(a, dim, 0) for a, dim in zip(arrays, dims)]
    widths = [t[0].size for t in turned]
    both = jnp.concatenate([t.reshape(-1, w) for t, w in zip(turned, widths)], axis=1)
    filled = lax.all_gather(both, axis, axis=0, tiled=True)
    parts = jnp.split(filled, [sum(widths[:k]) for k in range(1, len(widths))], axis=1)
    return tuple(
        (
            jnp.moveaxis(b.reshape(-1, *t.shape[1:]), 0, dim)
            for b, t, dim in zip(parts, turned, dims)
        )
    )


def contract(left_side, right_side):
    return lax.dot_general(
        left_side, right_side, (((0,), (0,)), ((), ())), preferred_element_type=jnp.float32
    )


def normed(stream, gain):
    whole_rows = gather_directly(stream, "tp", 0)
    values = whole_rows.astype(jnp.float32)
    inverse = lax.rsqrt(jnp.mean(values * values, axis=0) + EPS)
    return (values * inverse * gain[:, None]).astype(jnp.bfloat16)


def residual(stream, total, factor):
    return (stream.astype(jnp.float32) + factor * total).astype(jnp.bfloat16)


def swish_hidden(gate, gate_scale, upward, up_scale):
    return (jax.nn.silu(gate * gate_scale[:, None]) * (upward * up_scale[:, None])).astype(
        jnp.bfloat16
    )


def gating_unit(left_pre, right_pre, channel_gain, spatial, spatial_bias):
    left = jax.nn.gelu(left_pre)
    right = jax.nn.gelu(right_pre)
    totals, squares = in_one((jnp.sum(right, axis=0), jnp.sum(right * right, axis=0)), "tp")
    average = totals / BRANCH
    inverse = lax.rsqrt(squares / BRANCH - average * average + EPS)
    centred = ((right - average) * inverse * channel_gain[:, None]).astype(jnp.bfloat16)
    local_groups, span = (spatial.shape[0], spatial.shape[1])
    tokens = centred.shape[1]
    blocks = centred.reshape(local_groups, centred.shape[0] // local_groups, tokens // span, span)
    target = lax.broadcasted_iota(jnp.int32, (span, span), 0)
    source = lax.broadcasted_iota(jnp.int32, (span, span), 1)
    masked = jnp.where((source <= target)[None], spatial, jnp.zeros_like(spatial))
    token_mix = jnp.einsum("gts,gcns->gcnt", masked, blocks, preferred_element_type=jnp.float32)
    token_mix = token_mix + spatial_bias[:, None, None, :]
    return (left * token_mix.reshape(centred.shape[0], tokens)).astype(jnp.bfloat16)


def reduce_whole(weight_full, scale_full, hidden):
    return summed_on_arrival(
        (contract(weight_full, hidden) * scale_full[:, None]).astype(jnp.bfloat16), "tp", 0
    )


def local(
    stream,
    first_gain,
    first_gate,
    first_gate_scale,
    first_up,
    first_up_scale,
    first_down,
    first_down_scale,
    mixer_gain,
    mixer_left,
    mixer_left_scale,
    mixer_right,
    mixer_right_scale,
    channel_gain,
    spatial,
    spatial_bias,
    mixer_out,
    mixer_out_scale,
    second_gain,
    second_gate,
    second_gate_scale,
    second_up,
    second_up_scale,
    second_down,
    second_down_scale,
):
    first_cols, mixer_cols, second_cols = turned_gather(
        (first_down_scale, mixer_out_scale, second_down_scale), "fs", (0, 0, 0)
    )
    bf = jnp.bfloat16
    collected = turned_gather(
        (
            first_gate.astype(bf),
            first_up.astype(bf),
            first_down.astype(bf),
            mixer_left.astype(bf),
            mixer_right.astype(bf),
            mixer_out.astype(bf),
            second_gate.astype(bf),
            second_up.astype(bf),
            second_down.astype(bf),
        ),
        "fs",
        (0, 0, 1, 0, 0, 1, 0, 0, 1),
    )
    first_rows = normed(stream, first_gain)
    hidden = swish_hidden(
        contract(collected[0], first_rows),
        first_gate_scale,
        contract(collected[1], first_rows),
        first_up_scale,
    )
    stream = residual(stream, reduce_whole(collected[2], first_cols, hidden), 0.5)
    mixer_rows = normed(stream, mixer_gain)
    left_pre = contract(collected[3], mixer_rows) * mixer_left_scale[:, None]
    right_pre = contract(collected[4], mixer_rows) * mixer_right_scale[:, None]
    gated = gating_unit(left_pre, right_pre, channel_gain, spatial, spatial_bias)
    stream = residual(stream, reduce_whole(collected[5], mixer_cols, gated), 1.0)
    second_rows = normed(stream, second_gain)
    hidden = swish_hidden(
        contract(collected[6], second_rows),
        second_gate_scale,
        contract(collected[7], second_rows),
        second_up_scale,
    )
    stream = residual(stream, reduce_whole(collected[8], second_cols, hidden), 0.5)
    return stream


def solution(mesh):
    return jax.shard_map(
        local,
        mesh=mesh,
        in_specs=(
            P("tp", ("grp", "fs")),
            P(),
            P("fs", "tp"),
            P("tp"),
            P("fs", "tp"),
            P("tp"),
            P("tp", "fs"),
            P("fs"),
            P(),
            P("fs", "tp"),
            P("tp"),
            P("fs", "tp"),
            P("tp"),
            P("tp"),
            P("tp", None, None),
            P("tp", None),
            P("tp", "fs"),
            P("fs"),
            P(),
            P("fs", "tp"),
            P("tp"),
            P("fs", "tp"),
            P("tp"),
            P("tp", "fs"),
            P("fs"),
        ),
        out_specs=P("tp", ("grp", "fs")),
        check_vma=False,
    )
```

profile of v0, /device:TPU:33, one launch (start us, length us, event | category | flops | bytes accessed | tf_op | source)
XLA Modules:
  0.0 418.8 jit_solution(11805222702102936136)
XLA Ops:
  6.6 0.1 all-gather.2.cloned.1.call-start
  6.6 1.0 copy.40
  7.7 1.0 copy.41
  8.6 1.0 convert_dynamic-update-slice_fusion.3
  9.6 1.0 convert_dynamic-update-slice_fusion.2
  10.6 1.0 bitcast_dynamic-update-slice_fusion.1
  11.7 0.0 copy-start.1
  11.7 0.0 copy-done.5
  11.7 0.0 copy-done.2
  11.8 0.0 copy-done.3
  11.8 0.0 copy-done.4
  11.9 0.0 copy-start
  11.9 1.0 copy-done
  12.9 0.1 all-gather.2.cloned.1.call-update
  13.0 0.0 copy-done.1
  13.0 1.3 broadcast_in_dim.10
  14.3 24.0 %all-to-all-start = ((bf16[8,256,384]{2,1,0:T(8,128)(2,1)}), bf16[8,256,384]{2,1,0:T(8,128)(2,1)S(1)}, u32[]{:S(2)}, u32[]{:S(2)}) async-start(bf16[8,256,384]{2,1,0:T(8,128)(2,1)} %broadcast_in_dim.10), calls=%async_computation | async-start | bytes 3145728 | tf_op jit(solution)/shard_map/all_to_all | solution.py:20
  38.3 0.0 copy-done.12
  38.3 0.0 copy-done.13
  38.3 0.0 copy-done.14
  38.4 26.9 %all_gather.7 = f32[2048,3]{0,1:T(4,128)S(1)} all-gather(f32[128,3]{0,1:T(4,128)S(1)} %pad_maximum_fusion.1), channel_id=1, replica_groups=mesh['grp'=2,'fs'=16,'tp'=8] {'fs'}, dimensions={0}, use_global_device_ids=true | all-gather | bytes 26112 | tf_op jit(solution)/shard_map/all_gather | solution.py:56
  65.3 0.0 all-to-all-done
  65.3 0.4 multiply_reduce_fusion.2
  65.7 0.0 copy-done.7
  65.7 0.0 copy-start.15
  65.7 0.4 fusion.5
  66.1 0.0 copy-start.16
  66.1 176.1 %all-gather.2.cloned.1.call-done = bf16[2048,4608]{0,1:T(8,128)(2,1)} async-done(((bf16[128,4608]{0,1:T(8,128)(2,1)}), bf16[2048,4608]{0,1:T(8,128)(2,1)}) %all-gather.2.cloned.1.call-update) | async-done | bytes 18874384 | tf_op jit(solution)/shard_map/all_gather | solution.py:56
  242.2 4.5 %fusion.16 = f32[704,384]{1,0:T(8,128)} fusion(bf16[2048,384]{1,0:T(8,128)(2,1)S(1)} %fusion.5, bf16[2048,4608]{0,1:T(8,128)(2,1)} %all-gather.2.cloned.1.call-done, f32[704]{0:T(1024)S(1)} %copy-done.15), kind=kOutput, calls=%fused_computation.28 | convolution fusion | flops 1107566592 | bytes 5540608 | tf_op jit(solution)/shard_map/dot_general | solution.py:67
  246.7 0.0 copy-done.16
  246.7 6.3 %multiply_convert_fusion.2 = bf16[2048,384]{1,0:T(8,128)(2,1)S(1)} fusion(bf16[2048,4608]{0,1:T(8,128)(2,1)} %all-gather.2.cloned.1.call-done, f32[2048]{0:T(1024)S(1)} %bitcast.54, bf16[2048,384]{1,0:T(8,128)(2,1)S(1)} %fusion.5, f32[704,384]{1,0:T(8,128)} %fusion.16, f32[704]{0:T(1024)S(1)} %copy-done.16), kind=kOutput, calls=%fused_computation.16 | convolution fusion | flops 2218057728 | bytes 10005248 | tf_op jit(solution)/shard_map/dot_general | solution.py:67
  253.0 34.8 %all_to_all.36 = bf16[8,256,384]{2,1,0:T(8,128)(2,1)S(1)} all-to-all(bf16[8,256,384]{2,1,0:T(8,128)(2,1)S(1)} %bitcast.48), channel_id=1, replica_groups=mesh['grp'=2,'fs'=16,'tp'=8] {'tp'}, dimensions={0} | all-to-all | bytes 3145728 | tf_op jit(solution)/shard_map/all_to_all | solution.py:48
  287.8 0.2 convert_reduce_fusion.2
  288.0 0.1 add_convert_fusion.2
  288.1 0.1 broadcast_in_dim.11
  288.2 24.1 %all_to_all.37 = bf16[8,256,384]{2,1,0:T(8,128)(2,1)S(1)} all-to-all(bf16[8,256,384]{2,1,0:T(8,128)(2,1)S(1)} %broadcast_in_dim.11), channel_id=1, replica_groups=mesh['grp'=2,'fs'=16,'tp'=8] {'tp'}, dimensions={0} | all-to-all | bytes 3145728 | tf_op jit(solution)/shard_map/all_to_all | solution.py:20
  312.3 0.4 multiply_reduce_fusion.1
  312.7 0.3 copy-done.8
  313.0 0.4 fusion.3
  313.4 0.2 copy-done.19
  313.7 1.6 fusion.99
  315.3 8.1 %all_to_all.38 = f32[8,1,768]{2,1,0:T(1,128)S(1)} all-to-all(f32[8,1,768]{2,1,0:T(1,128)S(1)} %broadcast_in_dim.12), channel_id=1, replica_groups=mesh['grp'=2,'fs'=16,'tp'=8] {'tp'}, dimensions={0} | all-to-all | bytes 49152 | tf_op jit(solution)/shard_map/all_to_all | solution.py:20
  323.5 0.0 copy-done.10
  323.5 0.1 multiply_convert_fusion.3
  323.6 0.1 copy.43
  323.7 0.0 copy-done.6
  323.7 0.0 copy-done.11
  323.7 0.2 convolution_add_fusion
  323.9 0.1 copy.45
  324.0 2.2 multiply_convert_fusion.1
  326.3 23.8 %all_to_all.39 = bf16[8,256,384]{2,1,0:T(8,128)(2,1)S(1)} all-to-all(bf16[8,256,384]{2,1,0:T(8,128)(2,1)S(1)} %bitcast.49), channel_id=1, replica_groups=mesh['grp'=2,'fs'=16,'tp'=8] {'tp'}, dimensions={0} | all-to-all | bytes 3145728 | tf_op jit(solution)/shard_map/all_to_all | solution.py:48
  350.1 0.2 convert_reduce_fusion.1
  350.3 0.1 add_convert_fusion.1
  350.3 0.1 broadcast_in_dim.14
  350.5 24.1 %all_to_all.40 = bf16[8,256,384]{2,1,0:T(8,128)(2,1)S(1)} all-to-all(bf16[8,256,384]{2,1,0:T(8,128)(2,1)S(1)} %broadcast_in_dim.14), channel_id=1, replica_groups=mesh['grp'=2,'fs'=16,'tp'=8] {'tp'}, dimensions={0} | all-to-all | bytes 3145728 | tf_op jit(solution)/shard_map/all_to_all | solution.py:20
  374.6 0.4 multiply_reduce_fusion
  375.0 0.3 copy-done.9
  375.3 0.4 fusion.1
  375.7 0.3 copy-done.17
  376.0 4.5 %fusion.25 = f32[704,384]{1,0:T(8,128)} fusion(bf16[2048,384]{1,0:T(8,128)(2,1)S(1)} %fusion.1, bf16[2048,4608]{0,1:T(8,128)(2,1)} %all-gather.2.cloned.1.call-done, f32[704]{0:T(1024)S(1)} %copy-done.17), kind=kOutput, calls=%fused_computation.31 | convolution fusion | flops 1107566592 | bytes 5540608 | tf_op jit(solution)/shard_map/dot_general | solution.py:67
  380.5 6.3 %multiply_convert_fusion = bf16[2048,384]{1,0:T(8,128)(2,1)S(1)} fusion(bf16[2048,4608]{0,1:T(8,128)(2,1)} %all-gather.2.cloned.1.call-done, f32[2048]{0:T(1024)S(1)} %bitcast.52, bf16[2048,384]{1,0:T(8,128)(2,1)S(1)} %fusion.1, f32[704,384]{1,0:T(8,128)} %fusion.25, f32[704]{0:T(1024)S(1)} %copy-done.18), kind=kOutput, calls=%fused_computation.10 | convolution fusion | flops 2218057728 | bytes 10005248 | tf_op jit(solution)/shard_map/dot_general | solution.py:67
  386.8 24.1 %all_to_all.41 = bf16[8,256,384]{2,1,0:T(8,128)(2,1)S(1)} all-to-all(bf16[8,256,384]{2,1,0:T(8,128)(2,1)S(1)} %bitcast.47), channel_id=1, replica_groups=mesh['grp'=2,'fs'=16,'tp'=8] {'tp'}, dimensions={0} | all-to-all | bytes 3145728 | tf_op jit(solution)/shard_map/all_to_all | solution.py:48
  410.9 0.2 convert_reduce_fusion
  411.2 0.7 add_convert_fusion
  (33 shorter events, 0.3 us)
Async XLA Ops:
  6.5 5.2 %copy-start.5 = (f32[128,128]{1,0:T(8,128)S(1)}, f32[128,128]{1,0:T(8,128)}, u32[]{:S(2)}) copy-start(f32[128,128]{1,0:T(8,128)} %param.41) | copy-start | bytes 196612
  6.5 5.2 %copy-start.2 = (f32[128,704]{0,1:T(8,128)S(1)}, f32[128,704]{0,1:T(8,128)}, u32[]{:S(2)}) copy-start(f32[128,704]{0,1:T(8,128)} %param.44) | copy-start | bytes 1081348
  6.6 5.2 %copy-start.3 = (f32[128,704]{0,1:T(8,128)S(1)}, f32[128,704]{0,1:T(8,128)}, u32[]{:S(2)}) copy-start(f32[128,704]{0,1:T(8,128)} %param.46) | copy-start | bytes 1081348
  6.6 5.3 %copy-start.4 = (f32[704,128]{1,0:T(8,128)S(1)}, f32[704,128]{1,0:T(8,128)}, u32[]{:S(2)}) copy-start(f32[704,128]{1,0:T(8,128)} %param.48) | copy-start | bytes 1081348
  6.6 235.6 %all-gather.2.cloned.1.call-start = ((), (), s32[]{:S(2)}) async-start(), calls=%async_computation.7 | async-start | bytes 20054016 | tf_op jit(solution)/shard_map/all_gather | solution.py:56
  11.7 1.3 copy-start.1
  11.9 1.0 copy-start
  14.3 24.1 %copy-start.12 = (f32[128]{0:T(128)S(1)}, f32[128]{0:T(128)}, u32[]{:S(2)}) copy-start(f32[128]{0:T(128)} %param.49) | copy-start | bytes 1540
  14.3 24.1 %copy-start.13 = (f32[128]{0:T(128)S(1)}, f32[128]{0:T(128)}, u32[]{:S(2)}) copy-start(f32[128]{0:T(128)} %param.42) | copy-start | bytes 1540
  14.3 24.1 %copy-start.14 = (f32[128]{0:T(128)S(1)}, f32[128]{0:T(128)}, u32[]{:S(2)}) copy-start(f32[128]{0:T(128)} %param.32) | copy-start | bytes 1540
  14.3 51.0 %all-to-all-start = ((bf16[8,256,384]{2,1,0:T(8,128)(2,1)}), bf16[8,256,384]{2,1,0:T(8,128)(2,1)S(1)}, u32[]{:S(2)}, u32[]{:S(2)}) async-start(bf16[8,256,384]{2,1,0:T(8,128)(2,1)} %broadcast_in_dim.10), calls=%async_computation | async-start | bytes 3145728 | tf_op jit(solution)/shard_map/all_to_all | solution.py:20
  38.3 27.4 %copy-start.7 = (f32[2048]{0:T(1024)S(1)}, f32[2048]{0:T(1024)}, u32[]{:S(2)}) copy-start(f32[2048]{0:T(1024)} %param.26) | copy-start | bytes 24580
  65.7 176.5 %copy-start.15 = (f32[704]{0:T(1024)S(1)}, f32[704]{0:T(1024)}, u32[]{:S(2)}) copy-start(f32[704]{0:T(1024)} %param.28) | copy-start | bytes 8452
  66.1 180.6 %copy-start.16 = (f32[704]{0:T(1024)S(1)}, f32[704]{0:T(1024)}, u32[]{:S(2)}) copy-start(f32[704]{0:T(1024)} %param.30) | copy-start | bytes 8452
  312.3 0.7 copy-start.8
  313.0 0.7 copy-start.19
  313.7 9.8 %copy-start.10 = (f32[128]{0:T(128)S(1)}, f32[128]{0:T(128)}, u32[]{:S(2)}) copy-start(f32[128]{0:T(128)} %param.38) | copy-start | bytes 1540
  313.7 10.0 %copy-start.6 = (bf16[1,128,128]{2,1,0:T(8,128)(2,1)S(1)}, bf16[1,128,128]{2,1,0:T(8,128)(2,1)}, u32[]{:S(2)}) copy-start(bf16[1,128,128]{2,1,0:T(8,128)(2,1)} %param.39) | copy-start | bytes 98308
  313.7 10.0 %copy-start.11 = (f32[1,128]{1,0:T(1,128)S(1)}, f32[1,128]{1,0:T(1,128)}, u32[]{:S(2)}) copy-start(f32[1,128]{1,0:T(1,128)} %param.40) | copy-start | bytes 1540
  374.6 0.7 copy-start.9
  375.3 0.7 copy-start.17
  376.0 4.5 %copy-start.18 = (f32[704]{0:T(1024)S(1)}, f32[704]{0:T(1024)}, u32[]{:S(2)}) copy-start(f32[704]{0:T(1024)} %param.47) | copy-start | bytes 8452
Sparse Core Ops, SparseCore 0:
  13.1 229.0 all-gather.1
where the time goes:
time: 420 us; the launch traced here: 419 us
  waiting for transfers between devices  176 us (42%)
  blocking collectives  166 us (40%)
  matrix products  25.6 us (6%)
  starting transfers between devices  24.1 us (6%)
  between operations  13.7 us (3%)
  other arithmetic  7.33 us (2%)
  local copies, waits for them, and re-layouts  5.98 us (1%)
    all_gather x1, waiting for transfers between devices, turned_gather(): filled = lax.all_gather(both, axis, axis=0, tiled=True)  176 us
    all_to_all x3, blocking collectives, summed_on_arrival(): lax.all_to_all(parts, axis, split_axis=0, concat_axis=0, tiled=True)  82.7 us
    all_to_all x3, blocking collectives, copy_for_each(): return lax.all_to_all(copies, axis, split_axis=0, concat_axis=0, tiled=True)  56.4 us
    all_gather x1, blocking collectives, turned_gather(): filled = lax.all_gather(both, axis, axis=0, tiled=True)  26.9 us
    dot_general x6, matrix products, contract(): lax.dot_general(left_side, right_side, (((0,), (0,)), ((), ())), preferre...  25.4 us
    all_to_all x1, starting transfers between devices, copy_for_each(): return lax.all_to_all(copies, axis, split_axis=0, concat_axis=0, tiled=True)  24 us
  transfers between devices with their start and end apart: 2, of which 1 were waited for; matrix products, arithmetic and copies ran while one was open for 1% of the time, Pallas kernels for 0%

commit v1 on v0

v1 whole, which is shorter than its diff:
```python
import jax
import jax.numpy as jnp
from jax import lax
from jax.experimental import pallas as pl
from jax.experimental.pallas import tpu as pltpu
from jax.sharding import PartitionSpec as P

MESH = pl.DeviceIdType.MESH
EPS = 1e-06
F32, BF16 = jnp.float32, jnp.bfloat16
LANES = 128


def contract_rows(a, b):
    return lax.dot_general(a, b, (((0,), (0,)), ((), ())), preferred_element_type=F32)


def kernel(
    sizes,
    stream_ref,
    pack_ref,
    scale_ref,
    gains_ref,
    hidden_scales_ref,
    mixer_cols_ref,
    spatial_ref,
    bias_ref,
    out_ref,
    w,
    scl,
    act,
    xn,
    acc,
    hid,
    gated,
    left,
    right,
    pbuf,
    sb,
    pr,
    cb,
    rr,
    st,
    st_own,
    in_sem,
    zsend,
    zrecv,
    ssend,
    srecv,
    ysend,
    yrecv,
    psend,
    precv,
    csend,
    crecv,
    gsend,
    grecv,
    tsend,
    trecv,
):
    nz, ntp, ff, ch, span = sizes
    nx, half = ntp // 2, nz // 2
    rows, toks = stream_ref.shape
    g, z, t = lax.axis_index("grp"), lax.axis_index("fs"), lax.axis_index("tp")
    x, c = t // 2, t % 2
    gp = g % 2

    def at_tp(other):
        return (g, z, other)

    partner = (g + 1 - 2 * gp, z, t)
    sibling = at_tp(2 * x + 1 - c)
    xr, xl = (x + 1) % nx, (x + nx - 1) % nx
    right_x, left_x = at_tp(2 * xr + c), at_tp(2 * xl + c)
    around = ((g, (z + 1) % nz, t), (g, (z + nz - 1) % nz, t))

    def copy(src, dst, send, recv, device):
        return pltpu.make_async_remote_copy(
            src_ref=src, dst_ref=dst, send_sem=send, recv_sem=recv, device_id=device, device_id_type=MESH
        )

    third = ff * 15 // 44
    alone = (2 * third, third, ch, 2 * third, third)
    total = (2 * ff, ff, 3 * ch, 2 * ff, ff)
    base, first = [], 0
    for n in total:
        base.append(first)
        first += n

    def part(p, sub, zs):
        shared = total[p] - 2 * alone[p]
        if sub == 0:
            return w.at[zs, pl.ds(pl.multiple_of(base[p] + gp * (alone[p] + shared), 16), alone[p])]
        return w.at[zs, pl.ds(base[p] + alone[p], shared)]

    def other_part(p, zs):
        shared = total[p] - 2 * alone[p]
        return w.at[zs, pl.ds(pl.multiple_of(base[p] + (1 - gp) * (alone[p] + shared), 16), alone[p])]

    def source(d, k):
        return (z + nz - k) % nz if d == 0 else (z + k) % nz

    def last(d, sub):
        return half if d == sub else half - 1

    def hop(p, d, sub, zs, k):
        return copy(part(p, sub, zs), part(p, sub, zs), zsend.at[p, d, sub, k], zrecv.at[p, d, sub, k], around[d])

    def scale_hop(d, zs, k):
        return copy(scl.at[zs], scl.at[zs], ssend.at[d, k], srecv.at[d, k], around[d])

    def across(p, zs):
        return copy(part(p, 0, zs), part(p, 0, zs), ysend.at[p, zs], yrecv.at[p, zs], partner)

    def start_ring(p):
        for sub in (0, 1):
            for d in (0, 1):
                hop(p, d, sub, z, 0).start()

    def tick(p, k):
        for sub in (0, 1):
            for d in (0, 1):
                zs = source(d, k)

                @pl.when(k <= last(d, sub))
                def _():
                    hop(p, d, sub, zs, k - 1).wait_recv()

                @pl.when(k < last(d, sub))
                def _():
                    hop(p, d, sub, zs, k).start()

                if sub == 0:

                    @pl.when(k <= last(d, sub))
                    def _():
                        across(p, zs).start()

    def scale_tick(k):
        for d in (0, 1):
            zs = source(d, k)

            @pl.when(k <= last(d, 0))
            def _():
                scale_hop(d, zs, k - 1).wait_recv()

            @pl.when(k < last(d, 0))
            def _():
                scale_hop(d, zs, k).start()

    def pair_of(j):
        return (z + nz - j % half) % nz, (z + j) % nz

    def wait_across(p, j):
        for zs in pair_of(j):

            @pl.when(zs != z)
            def _():
                copy(other_part(p, zs), other_part(p, zs), ysend.at[p, zs], yrecv.at[p, zs], partner).wait_recv()

    own_rows = pl.ds(pl.multiple_of(t * rows, rows), rows)
    hr = rows // 2

    def chunk(r, tt, h):
        return act.at[r, pl.ds(pl.multiple_of(tt * rows + h * hr, hr), hr)]

    def g_half(r, i, tt, h, device):
        return copy(chunk(r, tt, h), chunk(r, tt, h), gsend.at[r, i], grecv.at[r, i], device)

    def g_whole(r):
        return copy(act.at[r, own_rows], act.at[r, own_rows], gsend.at[r, 0], grecv.at[r, 0], sibling)

    far = (x + 2) % nx

    def gather_start(r):
        g_half(r, 1, t, 0, right_x).start()
        g_half(r, 4, t, 1, left_x).start()
        g_half(r, 2, t, 1, right_x).start()
        g_half(r, 3, t, 0, left_x).start()
        g_whole(r).start()

    def gather_middle(r):
        from_left, from_right = 2 * xl + c, 2 * xr + c
        g_half(r, 1, from_left, 0, right_x).wait_recv()
        g_half(r, 5, from_left, 0, right_x).start()
        g_half(r, 7, from_left, 0, sibling).start()
        g_half(r, 4, from_right, 1, left_x).wait_recv()
        g_half(r, 6, from_right, 1, left_x).start()
        g_half(r, 10, from_right, 1, sibling).start()
        g_half(r, 2, from_left, 1, right_x).wait_recv()
        g_half(r, 8, from_left, 1, sibling).start()
        g_half(r, 3, from_right, 0, left_x).wait_recv()
        g_half(r, 9, from_right, 0, sibling).start()

    def gather_end(r):
        o = 1 - c
        g_half(r, 5, 2 * far + c, 0, right_x).wait_recv()
        g_half(r, 11, 2 * far + c, 0, sibling).start()
        g_half(r, 6, 2 * far + c, 1, left_x).wait_recv()
        g_half(r, 12, 2 * far + c, 1, sibling).start()
        g_whole(r).wait_recv()
        for i, xs, h in ((7, xl, 0), (8, xl, 1), (9, xr, 0), (10, xr, 1), (11, far, 0), (12, far, 1)):
            g_half(r, i, 2 * xs + o, h, sibling).wait_recv()

    def gather_drain(r):
        g_whole(r).wait_send()
        for i in range(1, 13):
            g_half(r, i, t, 0, sibling).wait_send()

    def normalise(r):
        def squares(i, s):
            v = act[r, pl.ds(pl.multiple_of(i * LANES, LANES), LANES)].astype(F32)
            return s + jnp.sum(v * v, axis=0, keepdims=True)

        s = lax.fori_loop(0, nz, squares, jnp.zeros((1, toks), F32))
        inverse = lax.rsqrt(s / (rows * ntp) + EPS)

        def apply(i, _):
            at = pl.ds(pl.multiple_of(i * LANES, LANES), LANES)
            v = act[r, at].astype(F32)
            xn[at] = (v * inverse * gains_ref[at, r : r + 1]).astype(BF16)
            return 0

        lax.fori_loop(0, nz, apply, 0)

    def project_pair(at, n, j, piece):
        a, b = pair_of(j)
        rhs = jnp.concatenate(
            [xn[pl.ds(pl.multiple_of(q * LANES, LANES), LANES)] for q in (a, b)], axis=0
        )

        def one(i, _):
            here = pl.ds(pl.multiple_of(at + i * piece, 16), piece)
            lhs = jnp.concatenate([w[a, here], w[b, here]], axis=1)
            got = jnp.dot(lhs, rhs, preferred_element_type=F32)
            there = pl.ds(pl.multiple_of(i * piece, 16), piece)
            acc[there] = acc[there] + got
            return 0

        lax.fori_loop(0, n // piece, one, 0)

    def clear(n):
        def one(i, _):
            acc[pl.ds(pl.multiple_of(i * 64, 64), 64)] = jnp.zeros((64, toks), F32)
            return 0

        lax.fori_loop(0, n // 64, one, 0)

    def hidden(b):
        def one(i, _):
            at = pl.ds(pl.multiple_of(i * 64, 64), 64)
            up_at = pl.ds(pl.multiple_of(ff + i * 64, 64), 64)
            gate = acc[at] * hidden_scales_ref[at, 2 * b : 2 * b + 1]
            up = acc[up_at] * hidden_scales_ref[at, 2 * b + 1 : 2 * b + 2]
            hid[at] = (gate / (1.0 + jnp.exp(-gate)) * up).astype(BF16)
            return 0

        lax.fori_loop(0, ff // 64, one, 0)

    def to_sibling(r, zs):
        return copy(sb.at[r, zs], pr.at[r, zs], psend.at[r, zs], precv.at[r, zs], sibling)

    def to_owner(r, zs):
        return copy(
            cb.at[r, zs],
            rr.at[r, x, zs % 2],
            csend.at[r, zs],
            crecv.at[r, x, zs % 2],
            at_tp(2 * (zs // 4) + c),
        )

    def produce(r, j, lhs, rhs):
        product = contract_rows(lhs, rhs)
        for i, zs in enumerate(pair_of(j)):
            col = jnp.transpose(scl[zs])[:, r : r + 1]
            term = product[i * LANES : (i + 1) * LANES] * col
            mine = (zs // 2) % 2 == c

            @pl.when(mine)
            def _():
                pbuf[zs] = term

            @pl.when(jnp.logical_not(mine))
            def _():
                sb[r, zs] = term.astype(BF16)
                to_sibling(r, zs).start()

    def combine(r, j):
        for zs in pair_of(j):

            @pl.when((zs // 2) % 2 == c)
            def _():
                to_sibling(r, zs).wait_recv()
                both = (pbuf[zs] + pr[r, zs].astype(F32)).astype(BF16)

                @pl.when(zs // 4 == x)
                def _():
                    rr[r, x, zs % 2] = both

                @pl.when(zs // 4 != x)
                def _():
                    cb[r, zs] = both
                    to_owner(r, zs).start()

    def finish(r, factor):
        for xs in range(nx):

            @pl.when(xs != x)
            def _():
                for h in (0, 1):
                    copy(cb.at[r, 0], rr.at[r, xs, h], csend.at[r, 0], crecv.at[r, xs, h], sibling).wait_recv()

        news = []
        for h in (0, 1):
            summed = rr[r, 0, h].astype(F32)
            for xs in range(1, nx):
                summed = summed + rr[r, xs, h].astype(F32)
            at = pl.ds(pl.multiple_of(t * rows + h * LANES, LANES), LANES)
            news.append((act[r, at].astype(F32) + factor * summed).astype(BF16))
        return news

    def next_stream(r, factor):
        for h, new in enumerate(finish(r, factor)):
            act[r + 1, pl.ds(pl.multiple_of(t * rows + h * LANES, LANES), LANES)] = new

    def reduce_drain(r):
        def one(zs, _):
            @pl.when((zs // 2) % 2 != c)
            def _():
                to_sibling(r, zs).wait_send()

            @pl.when(jnp.logical_and((zs // 2) % 2 == c, zs // 4 != x))
            def _():
                to_owner(r, zs).wait_send()

            return 0

        lax.fori_loop(0, nz, one, 0)

    def down_piece(p, r, j):
        a, b = pair_of(j)
        lhs = jnp.concatenate([w[a, pl.ds(base[p], ff)], w[b, pl.ds(base[p], ff)]], axis=1)
        produce(r, j, lhs, hid[...])

    fetch_stream = pltpu.make_async_copy(stream_ref, act.at[0, own_rows], in_sem.at[0])
    fetch_scale = pltpu.make_async_copy(scale_ref, scl.at[z], in_sem.at[1])
    fetches = [
        pltpu.make_async_copy(
            pack_ref.at[pl.ds(base[p], total[p])], w.at[z, pl.ds(base[p], total[p])], in_sem.at[2 + p]
        )
        for p in range(5)
    ]
    fetches[0].start()
    fetch_stream.start()
    fetch_scale.start()
    for p in range(1, 5):
        fetches[p].start()

    barrier = pltpu.get_barrier_semaphore()
    peers = [*around, partner] + [at_tp((t + d) % ntp) for d in range(1, ntp)]
    for device in peers:
        pl.semaphore_signal(barrier, inc=1, device_id=device, device_id_type=MESH)
    pl.semaphore_wait(barrier, len(peers))

    fetches[0].wait()
    start_ring(0)
    fetch_stream.wait()
    gather_start(0)
    fetch_scale.wait()
    for d in (0, 1):
        scale_hop(d, z, 0).start()
    for p in range(1, 5):
        fetches[p].wait()
    clear(2 * ff)
    tick(0, 1)
    gather_middle(0)
    scale_tick(1)
    tick(0, 2)
    gather_end(0)
    normalise(0)

    def first_loop(j, _):
        @pl.when(j + 2 <= half)
        def _():
            tick(0, j + 2)
            scale_tick(j + 1)

        @pl.when(j + 2 == half - 1)
        def _():
            start_ring(1)
            start_ring(2)

        wait_across(0, j)
        project_pair(base[0], 2 * ff, j, ff // 2)
        return 0

    lax.fori_loop(1, half + 1, first_loop, 0)
    scale_tick(half)
    hidden(0)
    tick(1, 1)
    tick(2, 1)

    def second_loop(j, _):
        @pl.when(j + 1 <= half)
        def _():
            tick(1, j + 1)
            tick(2, j + 1)

        @pl.when(j + 1 == half - 1)
        def _():
            start_ring(3)

        wait_across(1, j)
        down_piece(1, 0, j)

        @pl.when(j > 1)
        def _():
            combine(0, j - 1)

        return 0

    lax.fori_loop(1, half + 1, second_loop, 0)
    combine(0, half)
    tick(3, 1)
    next_stream(0, 0.5)
    gather_start(1)
    tick(3, 2)
    gather_middle(1)
    tick(3, 3)
    gather_end(1)
    normalise(1)
    clear(2 * ch)

    def mixer_loop(j, _):
        wait_across(2, j)
        project_pair(base[2], 2 * ch, j, 2 * ch)
        return 0

    lax.fori_loop(1, half + 1, mixer_loop, 0)
    left[...] = jax.nn.gelu(acc[0:ch] * mixer_cols_ref[:, 0:1])
    right[...] = jax.nn.gelu(acc[ch : 2 * ch] * mixer_cols_ref[:, 1:2])
    st_own[...] = jnp.zeros_like(st_own)
    st_own[0:1] = jnp.sum(right[...], axis=0, keepdims=True)
    st_own[1:2] = jnp.sum(right[...] * right[...], axis=0, keepdims=True)

    def to_peer(d):
        return copy(st_own, st.at[t], tsend.at[d - 1], trecv.at[t], at_tp((t + d) % ntp))

    def from_peer(d):
        src = (t + d) % ntp
        return copy(st_own, st.at[src], tsend.at[d - 1], trecv.at[src], at_tp(src))

    for d in range(1, ntp):
        to_peer(d).start()
    tick(3, 4)
    st[t] = st_own[...]
    for d in range(1, ntp):
        from_peer(d).wait_recv()
    sums = st[0]
    for i in range(1, ntp):
        sums = sums + st[i]
    average = sums[0:1] / (ch * ntp)
    inverse = lax.rsqrt(sums[1:2] / (ch * ntp) - average * average + EPS)
    centred = ((right[...] - average) * inverse * mixer_cols_ref[:, 2:3]).astype(BF16)
    target = lax.broadcasted_iota(jnp.int32, (span, span), 0)
    origin = lax.broadcasted_iota(jnp.int32, (span, span), 1)
    masked = jnp.where(origin <= target, spatial_ref[...].astype(F32), 0.0).astype(BF16)
    for n in range(toks // span):
        at = slice(n * span, (n + 1) * span)
        mixed = lax.dot_general(
            centred[:, at], masked, (((1,), (1,)), ((), ())), preferred_element_type=F32
        )
        gated[:, at] = (left[:, at] * (mixed + bias_ref[...])).astype(BF16)

    def mixer_out_loop(j, _):
        a, b = pair_of(j)
        here = pl.ds(base[2] + 2 * ch, ch)
        produce(1, j, jnp.concatenate([w[a, here], w[b, here]], axis=1), gated[...])

        @pl.when(j > 1)
        def _():
            combine(1, j - 1)

        return 0

    lax.fori_loop(1, half + 1, mixer_out_loop, 0)
    combine(1, half)
    tick(3, 5)
    next_stream(1, 1.0)
    gather_start(2)
    tick(3, 6)
    gather_middle(2)
    start_ring(4)
    tick(3, 7)
    gather_end(2)
    normalise(2)
    clear(2 * ff)
    tick(3, 8)
    early = 3

    def third_loop(j, _):
        @pl.when(j % 2 == 1)
        def _():
            @pl.when((j + 1) // 2 <= early)
            def _():
                tick(4, (j + 1) // 2)

        wait_across(3, j)
        project_pair(base[3], 2 * ff, j, ff // 2)
        return 0

    lax.fori_loop(1, half + 1, third_loop, 0)
    hidden(1)

    def fourth_loop(j, _):
        @pl.when(j + early <= half)
        def _():
            tick(4, j + early)

        wait_across(4, j)
        down_piece(4, 2, j)

        @pl.when(j > 1)
        def _():
            combine(2, j - 1)

        return 0

    lax.fori_loop(1, half + 1, fourth_loop, 0)
    combine(2, half)
    for h, new in enumerate(finish(2, 0.5)):
        out_ref[h * LANES : (h + 1) * LANES] = new

    def drain(k, _):
        for p in range(5):
            for sub in (0, 1):
                for d in (0, 1):

                    @pl.when(k < last(d, sub))
                    def _():
                        hop(p, d, sub, z, k).wait_send()

            for zs in (2 * k, 2 * k + 1):

                @pl.when(zs != z)
                def _():
                    across(p, zs).wait_send()
        for d in (0, 1):

            @pl.when(k < last(d, 0))
            def _():
                scale_hop(d, z, k).wait_send()

        return 0

    lax.fori_loop(0, half, drain, 0)
    for r in range(3):
        gather_drain(r)
        reduce_drain(r)
    for d in range(1, ntp):
        to_peer(d).wait_send()


def solution(mesh):
    nz, ntp = mesh.shape["fs"], mesh.shape["tp"]

    def local(
        stream,
        first_gain,
        first_gate,
        first_gate_scale,
        first_up,
        first_up_scale,
        first_down,
        first_down_scale,
        mixer_gain,
        mixer_left,
        mixer_left_scale,
        mixer_right,
        mixer_right_scale,
        channel_gain,
        spatial,
        spatial_bias,
        mixer_out,
        mixer_out_scale,
        second_gain,
        second_gate,
        second_gate_scale,
        second_up,
        second_up_scale,
        second_down,
        second_down_scale,
    ):
        rows, toks = stream.shape
        width, ff = first_gate.shape
        ch, span = mixer_left.shape[1], spatial.shape[1]
        whole = width * nz
        pack = jnp.concatenate(
            [
                first_gate.T,
                first_up.T,
                first_down,
                mixer_left.T,
                mixer_right.T,
                mixer_out,
                second_gate.T,
                second_up.T,
                second_down,
            ],
            axis=0,
        ).astype(BF16)
        scales = jnp.stack([first_down_scale, mixer_out_scale, second_down_scale] + [second_down_scale] * 5)
        gains = jnp.stack([first_gain, mixer_gain, second_gain], axis=1)
        hidden_scales = jnp.stack(
            [first_gate_scale, first_up_scale, second_gate_scale, second_up_scale], axis=1
        )
        mixer_cols = jnp.stack([mixer_left_scale, mixer_right_scale, channel_gain], axis=1)
        depth = pack.shape[0]
        dma, half = pltpu.SemaphoreType.DMA, nz // 2
        vmem, anywhere = pl.BlockSpec(memory_space=pltpu.VMEM), pl.BlockSpec(memory_space=pl.ANY)
        sizes = (nz, ntp, ff, ch, span)

        def body(*refs):
            kernel(sizes, *refs)

        piece = (nz, LANES, toks)
        return pl.pallas_call(
            body,
            out_shape=jax.ShapeDtypeStruct((rows, toks), BF16),
            in_specs=[anywhere, anywhere, anywhere] + [vmem] * 5,
            out_specs=vmem,
            scratch_shapes=[
                pltpu.VMEM((nz, depth, LANES), BF16),
                pltpu.VMEM((nz, 8, LANES), F32),
                pltpu.VMEM((3, whole, toks), BF16),
                pltpu.VMEM((whole, toks), BF16),
                pltpu.VMEM((2 * ff, toks), F32),
                pltpu.VMEM((ff, toks), BF16),
                pltpu.VMEM((ch, toks), BF16),
                pltpu.VMEM((ch, toks), F32),
                pltpu.VMEM((ch, toks), F32),
                pltpu.VMEM(piece, F32),
                pltpu.VMEM((3, *piece), BF16),
                pltpu.VMEM((3, *piece), BF16),
                pltpu.VMEM((3, *piece), BF16),
                pltpu.VMEM((3, ntp // 2, 2, LANES, toks), BF16),
                pltpu.VMEM((ntp, 8, toks), F32),
                pltpu.VMEM((8, toks), F32),
                dma((7,)),
                dma((5, 2, 2, half)),
                dma((5, 2, 2, half)),
                dma((2, half)),
                dma((2, half)),
                dma((5, nz)),
                dma((5, nz)),
                dma((3, nz)),
                dma((3, nz)),
                dma((3, nz)),
                dma((3, ntp // 2, 2)),
                dma((3, 13)),
                dma((3, 13)),
                dma((ntp,)),
                dma((ntp,)),
            ],
            compiler_params=pltpu.CompilerParams(
                collective_id=0, has_side_effects=True, vmem_limit_bytes=60 * 1024 * 1024
            ),
            name="layer",
        )(stream, pack, scales, gains, hidden_scales, mixer_cols, spatial.reshape(span, span), spatial_bias)

    return jax.shard_map(
        local,
        mesh=mesh,
        in_specs=(
            P("tp", ("grp", "fs")),
            P(),
            P("fs", "tp"),
            P("tp"),
            P("fs", "tp"),
            P("tp"),
            P("tp", "fs"),
            P("fs"),
            P(),
            P("fs", "tp"),
            P("tp"),
            P("fs", "tp"),
            P("tp"),
            P("tp"),
            P("tp", None, None),
            P("tp", None),
            P("tp", "fs"),
            P("fs"),
            P(),
            P("fs", "tp"),
            P("tp"),
            P("fs", "tp"),
            P("tp"),
            P("tp", "fs"),
            P("fs"),
        ),
        out_specs=P("tp", ("grp", "fs")),
        check_vma=False,
    )
```

time: 420 us -> 222 us (0.53)
  Pallas kernels: 0 us -> 211 us
  waiting for transfers between devices: 176 us -> 0 us
  blocking collectives: 166 us -> 0 us
  matrix products: 25.6 us -> 0 us
  starting transfers between devices: 24.1 us -> 0 us
  between operations: 13.7 us -> 0.34 us
  other arithmetic: 7.33 us -> 2.36 us
    pallas_call x0 -> x1, Pallas kernels: none -> 211 us  [local(): pl.pallas_call(body, out_shape=jax.ShapeDtypeStruct((rows, toks), BF16),...]
    all_gather x1 -> x0, waiting for transfers between devices: 176 us -> none  [turned_gather(): filled = lax.all_gather(both, axis, axis=0, tiled=True)]
    all_to_all x6 -> x0, blocking collectives: 139 us -> none  [the longest x3 82.7 us: summed_on_arrival(): lax.all_to_all(parts, axis, split_axis=0, concat_axis=0, tiled=True)]
    all_gather x1 -> x0, blocking collectives: 26.9 us -> none  [turned_gather(): filled = lax.all_gather(both, axis, axis=0, tiled=True)]
    dot_general x7 -> x0, matrix products: 25.6 us -> none  [the longest x6 25.4 us: contract(): lax.dot_general(left_side, right_side, (((0,), (0,)), ((), ())), preferre...]
    all_to_all x1 -> x0, starting transfers between devices: 24 us -> none  [copy_for_each(): return lax.all_to_all(copies, axis, split_axis=0, concat_axis=0, tiled=True)]
  transfers between devices with their start and end apart: 2 -> 0, of which waited for: 1 -> 0; matrix products, arithmetic and copies ran while one was open for 1% -> 0% of each run, Pallas kernels for 0% -> 0%
where the time goes in v1:
time: 222 us; the launch traced here: 220 us
  Pallas kernels  211 us (95%)
  local copies, waits for them, and re-layouts  5.67 us (3%)
  other arithmetic  2.36 us (1%)
    pallas_call x1, Pallas kernels, local(): pl.pallas_call(body, out_shape=jax.ShapeDtypeStruct((rows, toks), BF16),...  211 us

profile of v1, /device:TPU:33, one launch (start us, length us, event | category | flops | bytes accessed | tf_op | source)
XLA Modules:
  0.0 219.7 jit_solution(10060538292297174016)
XLA Ops:
  0.0 0.0 copy-start.1
  0.0 0.0 copy-start.5
  0.0 0.0 copy-start.6
  0.0 0.0 copy-start.7
  0.0 0.0 copy-start.2
  0.0 0.0 copy-start.3
  0.0 1.1 bitcast_dynamic-update-slice_fusion.3
  1.1 0.0 copy-start.4
  1.2 1.1 bitcast_dynamic-update-slice_fusion.2
  2.2 0.0 copy-done.1
  2.2 0.0 copy-start.9
  2.2 0.0 copy-start.10
  2.3 0.0 copy-start.11
  2.3 0.0 copy-done.5
  2.3 0.1 copy.43
  2.4 0.0 copy-done.6
  2.5 0.1 copy.44
  2.6 0.0 copy-done.7
  2.6 0.0 copy-done.2
  2.7 0.0 copy-done.3
  2.7 0.0 copy-start.12
  2.7 0.0 copy-start.13
  2.7 0.0 copy-start.14
  2.7 0.0 copy-start.15
  2.8 0.0 copy-done.4
  2.8 0.0 copy-start.16
  2.8 0.0 copy-start.17
  2.8 0.0 copy-start.18
  2.8 0.0 copy-start.8
  2.8 0.0 copy-start.19
  2.8 0.0 copy-start.20
  2.9 0.0 copy-start
  2.9 0.1 copy-done.9
  2.9 0.0 copy-done.10
  3.0 0.0 copy-done.11
  3.0 1.3 copy.45.refs_3_
  4.3 0.0 copy-done.12
  4.3 0.0 copy-done.13
  4.4 0.0 copy-done.14
  4.4 0.0 copy-done.15
  4.4 0.9 copy.46.refs_4_
  5.4 0.0 copy-done.16
  5.4 0.0 copy-done.17
  5.4 0.0 copy-done.18
  5.4 0.7 copy.47.refs_5_
  6.1 0.0 copy-done.8
  6.1 0.0 copy-done.19
  6.1 0.0 copy-done.20
  6.1 0.6 stack.59.refs_2_
  6.7 0.0 copy-done
  6.7 211.3 %layer.1 = bf16[256,384]{1,0:T(8,128)(2,1)} custom-call(bf16[256,384]{1,0:T(8,128)(2,1)} %refs_0_.1, bf16[4608,128]{1,0:T(8,128)(2,1)} %copy-done, f32[8,128]{1,0:T(8,128)} %stack.59.refs_2_, f32[2048,3]{1,0:T(8,128)} %copy.45.refs_3_, f32[704,4]{1,0:T(8,128)} %copy.46.refs_4_, f32[128,3]{1,0:T(8,128)} %copy.47.refs_5_, bf16[128,128]{1,0:T(8,128)(2,1)} %bitcast.22, ...), custom_call_target="tpu_custom_call" | custom-call | tf_op jit(solution)/shard_map/layer/pallas_call | solution.py:627
  218.0 1.6 copy.57
  (14 shorter events, 0.2 us)
Async XLA Ops:
  0.0 2.2 %copy-start.1 = (f32[704,128]{1,0:T(8,128)S(1)}, f32[704,128]{1,0:T(8,128)}, u32[]{:S(2)}) copy-start(f32[704,128]{1,0:T(8,128)} %param.31) | copy-start | bytes 1081348
  0.0 2.3 %copy-start.5 = (f32[128,128]{1,0:T(8,128)S(1)}, f32[128,128]{1,0:T(8,128)}, u32[]{:S(2)}) copy-start(f32[128,128]{1,0:T(8,128)} %param.34) | copy-start | bytes 196612
  0.0 2.4 %copy-start.6 = (f32[128,128]{1,0:T(8,128)S(1)}, f32[128,128]{1,0:T(8,128)}, u32[]{:S(2)}) copy-start(f32[128,128]{1,0:T(8,128)} %param.36) | copy-start | bytes 196612
  0.0 2.6 %copy-start.7 = (f32[128,128]{1,0:T(8,128)S(1)}, f32[128,128]{1,0:T(8,128)}, u32[]{:S(2)}) copy-start(f32[128,128]{1,0:T(8,128)} %param.41) | copy-start | bytes 196612
  0.0 2.6 %copy-start.2 = (f32[128,704]{0,1:T(8,128)S(1)}, f32[128,704]{0,1:T(8,128)}, u32[]{:S(2)}) copy-start(f32[128,704]{0,1:T(8,128)} %param.44) | copy-start | bytes 1081348
  0.0 2.6 %copy-start.3 = (f32[128,704]{0,1:T(8,128)S(1)}, f32[128,704]{0,1:T(8,128)}, u32[]{:S(2)}) copy-start(f32[128,704]{0,1:T(8,128)} %param.46) | copy-start | bytes 1081348
  1.1 1.6 copy-start.4
  2.2 0.7 copy-start.9
  2.2 0.7 copy-start.10
  2.3 0.7 copy-start.11
  2.7 1.7 copy-start.12
  2.7 1.7 copy-start.13
  2.7 1.7 copy-start.14
  2.7 1.7 copy-start.15
  2.8 2.6 %copy-start.16 = (f32[128]{0:T(128)S(1)}, f32[128]{0:T(128)}, u32[]{:S(2)}) copy-start(f32[128]{0:T(128)} %param.38) | copy-start | bytes 1540
  2.8 2.6 %copy-start.17 = (f32[128]{0:T(128)S(1)}, f32[128]{0:T(128)}, u32[]{:S(2)}) copy-start(f32[128]{0:T(128)} %param.37) | copy-start | bytes 1540
  2.8 2.6 %copy-start.18 = (f32[128]{0:T(128)S(1)}, f32[128]{0:T(128)}, u32[]{:S(2)}) copy-start(f32[128]{0:T(128)} %param.35) | copy-start | bytes 1540
  2.8 3.3 %copy-start.8 = (f32[128]{0:T(128)S(1)}, f32[128]{0:T(128)}, u32[]{:S(2)}) copy-start(f32[128]{0:T(128)} %param.49) | copy-start | bytes 1540
  2.8 3.3 %copy-start.19 = (f32[128]{0:T(128)S(1)}, f32[128]{0:T(128)}, u32[]{:S(2)}) copy-start(f32[128]{0:T(128)} %param.32) | copy-start | bytes 1540
  2.8 3.3 %copy-start.20 = (f32[128]{0:T(128)S(1)}, f32[128]{0:T(128)}, u32[]{:S(2)}) copy-start(f32[128]{0:T(128)} %param.42) | copy-start | bytes 1540
  2.9 3.9 %copy-start = (bf16[4608,128]{1,0:T(8,128)(2,1)}, bf16[4608,128]{1,0:T(8,128)(2,1)S(1)}, u32[]{:S(2)}) copy-start(bf16[4608,128]{1,0:T(8,128)(2,1)S(1)} %convert_dynamic-update-slice_fusion.refs_1_) | copy-start | bytes 3538948

commit v2 on v1

--- a/solution.py
+++ b/solution.py
@@ -19,15 +19,13 @@
     sizes,
     stream_ref,
     pack_ref,
-    scale_ref,
-    gains_ref,
-    hidden_scales_ref,
-    mixer_cols_ref,
+    vectors_ref,
     spatial_ref,
     bias_ref,
     out_ref,
     w,
     scl,
+    cols,
     act,
     xn,
     acc,
@@ -60,6 +58,9 @@
 ):
     nz, ntp, ff, ch, span = sizes
     nx, half = ntp // 2, nz // 2
+    hidden_at = vectors_ref.shape[1] - 2 * LANES - (-ff % LANES) - ff
+    mixer_at = vectors_ref.shape[1] - 2 * LANES
+    scale_at = vectors_ref.shape[1] - LANES
     rows, toks = stream_ref.shape
     g, z, t = lax.axis_index("grp"), lax.axis_index("fs"), lax.axis_index("tp")
     x, c = t // 2, t % 2
@@ -93,10 +94,6 @@
             return w.at[zs, pl.ds(pl.multiple_of(base[p] + gp * (alone[p] + shared), 16), alone[p])]
         return w.at[zs, pl.ds(base[p] + alone[p], shared)]
 
-    def other_part(p, zs):
-        shared = total[p] - 2 * alone[p]
-        return w.at[zs, pl.ds(pl.multiple_of(base[p] + (1 - gp) * (alone[p] + shared), 16), alone[p])]
-
     def source(d, k):
         return (z + nz - k) % nz if d == 0 else (z + k) % nz
 
@@ -104,13 +101,13 @@
         return half if d == sub else half - 1
 
     def hop(p, d, sub, zs, k):
-        return copy(part(p, sub, zs), part(p, sub, zs), zsend.at[p, d, sub, k], zrecv.at[p, d, sub, k], around[d])
+        return copy(part(p, sub, zs), part(p, sub, zs), zsend.at[p], zrecv.at[p, d, sub, k], around[d])
 
     def scale_hop(d, zs, k):
-        return copy(scl.at[zs], scl.at[zs], ssend.at[d, k], srecv.at[d, k], around[d])
-
-    def across(p, zs):
-        return copy(part(p, 0, zs), part(p, 0, zs), ysend.at[p, zs], yrecv.at[p, zs], partner)
+        return copy(scl.at[zs], scl.at[zs], ssend.at[0], srecv.at[d, k], around[d])
+
+    def across(p, zs, k):
+        return copy(part(p, 0, zs), part(p, 0, zs), ysend.at[p], yrecv.at[p, k - 1], partner)
 
     def start_ring(p):
         for sub in (0, 1):
@@ -134,7 +131,7 @@
 
                     @pl.when(k <= last(d, sub))
                     def _():
-                        across(p, zs).start()
+                        across(p, zs, k).start()
 
     def scale_tick(k):
         for d in (0, 1):
@@ -152,11 +149,12 @@
         return (z + nz - j % half) % nz, (z + j) % nz
 
     def wait_across(p, j):
-        for zs in pair_of(j):
-
-            @pl.when(zs != z)
+        for several in (1, 2):
+
+            @pl.when((j < half) == (several == 2))
             def _():
-                copy(other_part(p, zs), other_part(p, zs), ysend.at[p, zs], yrecv.at[p, zs], partner).wait_recv()
+                pieces = w.at[pl.ds(0, several), pl.ds(base[p], alone[p])]
+                copy(pieces, pieces, ysend.at[p], yrecv.at[p, j - 1], partner).wait_recv()
 
     own_rows = pl.ds(pl.multiple_of(t * rows, rows), rows)
     hr = rows // 2
@@ -165,10 +163,10 @@
         return act.at[r, pl.ds(pl.multiple_of(tt * rows + h * hr, hr), hr)]
 
     def g_half(r, i, tt, h, device):
-        return copy(chunk(r, tt, h), chunk(r, tt, h), gsend.at[r, i], grecv.at[r, i], device)
+        return copy(chunk(r, tt, h), chunk(r, tt, h), gsend.at[r], grecv.at[r, i if i < 7 else 0], device)
 
     def g_whole(r):
-        return copy(act.at[r, own_rows], act.at[r, own_rows], gsend.at[r, 0], grecv.at[r, 0], sibling)
+        return copy(act.at[r, own_rows], act.at[r, own_rows], gsend.at[r], grecv.at[r, 0], sibling)
 
     far = (x + 2) % nx
 
@@ -193,19 +191,16 @@
         g_half(r, 9, from_right, 0, sibling).start()
 
     def gather_end(r):
-        o = 1 - c
         g_half(r, 5, 2 * far + c, 0, right_x).wait_recv()
         g_half(r, 11, 2 * far + c, 0, sibling).start()
         g_half(r, 6, 2 * far + c, 1, left_x).wait_recv()
         g_half(r, 12, 2 * far + c, 1, sibling).start()
-        g_whole(r).wait_recv()
-        for i, xs, h in ((7, xl, 0), (8, xl, 1), (9, xr, 0), (10, xr, 1), (11, far, 0), (12, far, 1)):
-            g_half(r, i, 2 * xs + o, h, sibling).wait_recv()
+        arrived = act.at[r, pl.ds(0, 4 * rows)]
+        copy(arrived, arrived, gsend.at[r], grecv.at[r, 0], sibling).wait_recv()
 
     def gather_drain(r):
-        g_whole(r).wait_send()
-        for i in range(1, 13):
-            g_half(r, i, t, 0, sibling).wait_send()
+        sent = act.at[r, pl.ds(0, 7 * rows)]
+        copy(sent, sent, gsend.at[r], grecv.at[r, 0], sibling).wait_send()
 
     def normalise(r):
         def squares(i, s):
@@ -218,7 +213,7 @@
         def apply(i, _):
             at = pl.ds(pl.multiple_of(i * LANES, LANES), LANES)
             v = act[r, at].astype(F32)
-            xn[at] = (v * inverse * gains_ref[at, r : r + 1]).astype(BF16)
+            xn[at] = (v * inverse * cols[at, r : r + 1]).astype(BF16)
             return 0
 
         lax.fori_loop(0, nz, apply, 0)
@@ -250,22 +245,23 @@
         def one(i, _):
             at = pl.ds(pl.multiple_of(i * 64, 64), 64)
             up_at = pl.ds(pl.multiple_of(ff + i * 64, 64), 64)
-            gate = acc[at] * hidden_scales_ref[at, 2 * b : 2 * b + 1]
-            up = acc[up_at] * hidden_scales_ref[at, 2 * b + 1 : 2 * b + 2]
+            scale = cols[pl.ds(pl.multiple_of(hidden_at + i * 64, 64), 64)]
+            gate = acc[at] * scale[:, 2 * b : 2 * b + 1]
+            up = acc[up_at] * scale[:, 2 * b + 1 : 2 * b + 2]
             hid[at] = (gate / (1.0 + jnp.exp(-gate)) * up).astype(BF16)
             return 0
 
         lax.fori_loop(0, ff // 64, one, 0)
 
     def to_sibling(r, zs):
-        return copy(sb.at[r, zs], pr.at[r, zs], psend.at[r, zs], precv.at[r, zs], sibling)
+        return copy(sb.at[r, zs], pr.at[r, zs], psend.at[r], precv.at[r, zs], sibling)
 
     def to_owner(r, zs):
         return copy(
             cb.at[r, zs],
             rr.at[r, x, zs % 2],
-            csend.at[r, zs],
-            crecv.at[r, x, zs % 2],
+            csend.at[r],
+            crecv.at[r],
             at_tp(2 * (zs // 4) + c),
         )
 
@@ -303,13 +299,8 @@
                     to_owner(r, zs).start()
 
     def finish(r, factor):
-        for xs in range(nx):
-
-            @pl.when(xs != x)
-            def _():
-                for h in (0, 1):
-                    copy(cb.at[r, 0], rr.at[r, xs, h], csend.at[r, 0], crecv.at[r, xs, h], sibling).wait_recv()
-
+        arrived = cb.at[r, pl.ds(0, 2 * (nx - 1))]
+        copy(arrived, arrived, csend.at[r], crecv.at[r], sibling).wait_recv()
         news = []
         for h in (0, 1):
             summed = rr[r, 0, h].astype(F32)
@@ -324,18 +315,10 @@
             act[r + 1, pl.ds(pl.multiple_of(t * rows + h * LANES, LANES), LANES)] = new
 
     def reduce_drain(r):
-        def one(zs, _):
-            @pl.when((zs // 2) % 2 != c)
-            def _():
-                to_sibling(r, zs).wait_send()
-
-            @pl.when(jnp.logical_and((zs // 2) % 2 == c, zs // 4 != x))
-            def _():
-                to_owner(r, zs).wait_send()
-
-            return 0
-
-        lax.fori_loop(0, nz, one, 0)
+        sent = sb.at[r, pl.ds(0, half)]
+        copy(sent, sent, psend.at[r], precv.at[r, 0], sibling).wait_send()
+        sent = cb.at[r, pl.ds(0, 2 * (nx - 1))]
+        copy(sent, sent, csend.at[r], crecv.at[r], sibling).wait_send()
 
     def down_piece(p, r, j):
         a, b = pair_of(j)
@@ -343,7 +326,9 @@
         produce(r, j, lhs, hid[...])
 
     fetch_stream = pltpu.make_async_copy(stream_ref, act.at[0, own_rows], in_sem.at[0])
-    fetch_scale = pltpu.make_async_copy(scale_ref, scl.at[z], in_sem.at[1])
+    fetch_scale = pltpu.make_async_copy(
+        vectors_ref.at[:, pl.ds(scale_at, LANES)], scl.at[z], in_sem.at[1]
+    )
     fetches = [
         pltpu.make_async_copy(
             pack_ref.at[pl.ds(base[p], total[p])], w.at[z, pl.ds(base[p], total[p])], in_sem.at[2 + p]
@@ -372,6 +357,13 @@
     for p in range(1, 5):
         fetches[p].wait()
     clear(2 * ff)
+
+    def turn(i, _):
+        at = pl.ds(pl.multiple_of(i * LANES, LANES), LANES)
+        cols[at] = jnp.transpose(vectors_ref[:, at])
+        return 0
+
+    lax.fori_loop(0, vectors_ref.shape[1] // LANES, turn, 0)
     tick(0, 1)
     gather_middle(0)
     scale_tick(1)
@@ -390,6 +382,11 @@
             start_ring(1)
             start_ring(2)
 
+        @pl.when(j == half)
+        def _():
+            tick(1, 1)
+            tick(2, 1)
+
         wait_across(0, j)
         project_pair(base[0], 2 * ff, j, ff // 2)
         return 0
@@ -397,8 +394,6 @@
     lax.fori_loop(1, half + 1, first_loop, 0)
     scale_tick(half)
     hidden(0)
-    tick(1, 1)
-    tick(2, 1)
 
     def second_loop(j, _):
         @pl.when(j + 1 <= half)
@@ -409,6 +404,7 @@
         @pl.when(j + 1 == half - 1)
         def _():
             start_ring(3)
+            start_ring(4)
 
         wait_across(1, j)
         down_piece(1, 0, j)
@@ -424,11 +420,13 @@
     tick(3, 1)
     next_stream(0, 0.5)
     gather_start(1)
+    tick(4, 1)
     tick(3, 2)
     gather_middle(1)
-    tick(3, 3)
+    tick(4, 2)
     gather_end(1)
     normalise(1)
+    tick(3, 3)
     clear(2 * ch)
 
     def mixer_loop(j, _):
@@ -437,31 +435,28 @@
         return 0
 
     lax.fori_loop(1, half + 1, mixer_loop, 0)
-    left[...] = jax.nn.gelu(acc[0:ch] * mixer_cols_ref[:, 0:1])
-    right[...] = jax.nn.gelu(acc[ch : 2 * ch] * mixer_cols_ref[:, 1:2])
+    mixer_cols = cols[mixer_at : mixer_at + ch]
+    left[...] = jax.nn.gelu(acc[0:ch] * mixer_cols[:, 0:1])
+    right[...] = jax.nn.gelu(acc[ch : 2 * ch] * mixer_cols[:, 1:2])
     st_own[...] = jnp.zeros_like(st_own)
     st_own[0:1] = jnp.sum(right[...], axis=0, keepdims=True)
     st_own[1:2] = jnp.sum(right[...] * right[...], axis=0, keepdims=True)
 
     def to_peer(d):
-        return copy(st_own, st.at[t], tsend.at[d - 1], trecv.at[t], at_tp((t + d) % ntp))
-
-    def from_peer(d):
-        src = (t + d) % ntp
-        return copy(st_own, st.at[src], tsend.at[d - 1], trecv.at[src], at_tp(src))
+        return copy(st_own, st.at[t], tsend.at[0], trecv.at[0], at_tp((t + d) % ntp))
 
     for d in range(1, ntp):
         to_peer(d).start()
-    tick(3, 4)
+    tick(4, 3)
     st[t] = st_own[...]
-    for d in range(1, ntp):
-        from_peer(d).wait_recv()
+    arrived = st.at[pl.ds(0, ntp - 1)]
+    copy(arrived, arrived, tsend.at[0], trecv.at[0], sibling).wait_recv()
     sums = st[0]
     for i in range(1, ntp):
         sums = sums + st[i]
     average = sums[0:1] / (ch * ntp)
     inverse = lax.rsqrt(sums[1:2] / (ch * ntp) - average * average + EPS)
-    centred = ((right[...] - average) * inverse * mixer_cols_ref[:, 2:3]).astype(BF16)
+    centred = ((right[...] - average) * inverse * mixer_cols[:, 2:3]).astype(BF16)
     target = lax.broadcasted_iota(jnp.int32, (span, span), 0)
     origin = lax.broadcasted_iota(jnp.int32, (span, span), 1)
     masked = jnp.where(origin <= target, spatial_ref[...].astype(F32), 0.0).astype(BF16)
@@ -477,88 +472,77 @@
         here = pl.ds(base[2] + 2 * ch, ch)
         produce(1, j, jnp.concatenate([w[a, here], w[b, here]], axis=1), gated[...])
 
-        @pl.when(j > 1)
-        def _():
-            combine(1, j - 1)
+        @pl.when(j > 2)
+        def _():
+            combine(1, j - 2)
+
+        @pl.when(j == half // 2)
+        def _():
+            tick(3, 4)
 
         return 0
 
     lax.fori_loop(1, half + 1, mixer_out_loop, 0)
+    tick(4, 4)
+    combine(1, half - 1)
     combine(1, half)
     tick(3, 5)
     next_stream(1, 1.0)
     gather_start(2)
+    tick(4, 5)
     tick(3, 6)
     gather_middle(2)
-    start_ring(4)
-    tick(3, 7)
+    tick(4, 6)
     gather_end(2)
     normalise(2)
     clear(2 * ff)
-    tick(3, 8)
-    early = 3
 
     def third_loop(j, _):
-        @pl.when(j % 2 == 1)
-        def _():
-            @pl.when((j + 1) // 2 <= early)
-            def _():
-                tick(4, (j + 1) // 2)
+        @pl.when(j == half - 3)
+        def _():
+            tick(3, half - 1)
+            tick(4, half - 1)
+
+        @pl.when(j == half - 1)
+        def _():
+            tick(3, half)
 
         wait_across(3, j)
         project_pair(base[3], 2 * ff, j, ff // 2)
         return 0
 
     lax.fori_loop(1, half + 1, third_loop, 0)
+    tick(4, half)
     hidden(1)
 
     def fourth_loop(j, _):
-        @pl.when(j + early <= half)
-        def _():
-            tick(4, j + early)
-
         wait_across(4, j)
         down_piece(4, 2, j)
 
-        @pl.when(j > 1)
-        def _():
-            combine(2, j - 1)
+        @pl.when(j > 2)
+        def _():
+            combine(2, j - 2)
 
         return 0
 
     lax.fori_loop(1, half + 1, fourth_loop, 0)
+    combine(2, half - 1)
     combine(2, half)
     for h, new in enumerate(finish(2, 0.5)):
         out_ref[h * LANES : (h + 1) * LANES] = new
 
-    def drain(k, _):
-        for p in range(5):
-            for sub in (0, 1):
-                for d in (0, 1):
-
-                    @pl.when(k < last(d, sub))
-                    def _():
-                        hop(p, d, sub, z, k).wait_send()
-
-            for zs in (2 * k, 2 * k + 1):
-
-                @pl.when(zs != z)
-                def _():
-                    across(p, zs).wait_send()
-        for d in (0, 1):
-
-            @pl.when(k < last(d, 0))
-            def _():
-                scale_hop(d, z, k).wait_send()
-
-        return 0
-
-    lax.fori_loop(0, half, drain, 0)
+    for p in range(5):
+        sent = w.at[pl.ds(0, nz - 1), pl.ds(base[p], total[p] - alone[p])]
+        copy(sent, sent, zsend.at[p], zrecv.at[p, 0, 0, 0], sibling).wait_send()
+        sent = w.at[pl.ds(0, nz - 1), pl.ds(base[p], alone[p])]
+        copy(sent, sent, ysend.at[p], yrecv.at[p, 0], sibling).wait_send()
+    sent = scl.at[pl.ds(0, nz - 1)]
+    copy(sent, sent, ssend.at[0], srecv.at[0, 0], sibling).wait_send()
     for r in range(3):
         gather_drain(r)
         reduce_drain(r)
-    for d in range(1, ntp):
-        to_peer(d).wait_send()
+    sent = st.at[pl.ds(0, ntp - 1)]
+    copy(sent, sent, tsend.at[0], trecv.at[0], sibling).wait_send()
 
 
 def solution(mesh):
@@ -609,12 +593,19 @@
             ],
             axis=0,
         ).astype(BF16)
-        scales = jnp.stack([first_down_scale, mixer_out_scale, second_down_scale] + [second_down_scale] * 5)
-        gains = jnp.stack([first_gain, mixer_gain, second_gain], axis=1)
-        hidden_scales = jnp.stack(
-            [first_gate_scale, first_up_scale, second_gate_scale, second_up_scale], axis=1
+
+        def eight_rows(*vectors):
+            return jnp.pad(jnp.stack(vectors), ((0, 8 - len(vectors)), (0, -vectors[0].shape[0] % LANES)))
+
+        vectors = jnp.concatenate(
+            [
+                eight_rows(first_gain, mixer_gain, second_gain),
+                eight_rows(first_gate_scale, first_up_scale, second_gate_scale, second_up_scale),
+                eight_rows(mixer_left_scale, mixer_right_scale, channel_gain),
+                eight_rows(first_down_scale, mixer_out_scale, second_down_scale),
+            ],
+            axis=1,
         )
-        mixer_cols = jnp.stack([mixer_left_scale, mixer_right_scale, channel_gain], axis=1)
         depth = pack.shape[0]
         dma, half = pltpu.SemaphoreType.DMA, nz // 2
         vmem, anywhere = pl.BlockSpec(memory_space=pltpu.VMEM), pl.BlockSpec(memory_space=pl.ANY)
@@ -627,11 +618,12 @@
         return pl.pallas_call(
             body,
             out_shape=jax.ShapeDtypeStruct((rows, toks), BF16),
-            in_specs=[anywhere, anywhere, anywhere] + [vmem] * 5,
+            in_specs=[anywhere, anywhere] + [vmem] * 3,
             out_specs=vmem,
             scratch_shapes=[
                 pltpu.VMEM((nz, depth, LANES), BF16),
                 pltpu.VMEM((nz, 8, LANES), F32),
+                pltpu.VMEM((vectors.shape[1], 8), F32),
                 pltpu.VMEM((3, whole, toks), BF16),
                 pltpu.VMEM((whole, toks), BF16),
                 pltpu.VMEM((2 * ff, toks), F32),
@@ -647,26 +639,26 @@
                 pltpu.VMEM((ntp, 8, toks), F32),
                 pltpu.VMEM((8, toks), F32),
                 dma((7,)),
+                dma((5,)),
                 dma((5, 2, 2, half)),
-                dma((5, 2, 2, half)),
+                dma((1,)),
                 dma((2, half)),
-                dma((2, half)),
-                dma((5, nz)),
-                dma((5, nz)),
+                dma((5,)),
+                dma((5, half)),
+                dma((3,)),
                 dma((3, nz)),
-                dma((3, nz)),
-                dma((3, nz)),
-                dma((3, ntp // 2, 2)),
-                dma((3, 13)),
-                dma((3, 13)),
-                dma((ntp,)),
-                dma((ntp,)),
+                dma((3,)),
+                dma((3,)),
+                dma((3,)),
+                dma((3, 7)),
+                dma((1,)),
+                dma((1,)),
             ],
             compiler_params=pltpu.CompilerParams(
                 collective_id=0, has_side_effects=True, vmem_limit_bytes=60 * 1024 * 1024
             ),
             name="layer",
-        )(stream, pack, scales, gains, hidden_scales, mixer_cols, spatial.reshape(span, span), spatial_bias)
+        )(stream, pack, vectors, spatial.reshape(span, span), spatial_bias)
 
     return jax.shard_map(
         local,

time: 222 us -> 198 us (0.89)
  Pallas kernels: 211 us -> 192 us
  local copies, waits for them, and re-layouts: 5.67 us -> 2.15 us
    pallas_call x1, Pallas kernels: 211 us -> 192 us  [local(): pl.pallas_call(body, out_shape=jax.ShapeDtypeStruct((rows, toks), BF16),...]
    another operation x8 -> x4, local copies, waits for them, and re-layouts: 3.62 us -> 0.01 us  [eight_rows(): jnp.stack(vectors)]
where the time goes in v2:
time: 198 us
  Pallas kernels  192 us (97%)
  other arithmetic  3.09 us (2%)
  local copies, waits for them, and re-layouts  2.15 us (1%)
    pallas_call x1, Pallas kernels, local(): pl.pallas_call(body, out_shape=jax.ShapeDtypeStruct((rows, toks), BF16),...  192 us

profile of v2, /device:TPU:33, one launch (start us, length us, event | category | flops | bytes accessed | tf_op | source)
XLA Modules:
  0.0 197.7 jit_solution(11329594707788954570)
XLA Ops:
  0.0 0.0 copy-start.1
  0.0 0.0 copy-start.5
  0.0 0.0 copy-start.6
  0.0 0.0 copy-start.7
  0.0 0.0 copy-start.2
  0.0 0.0 copy-start.3
  0.0 1.1 bitcast_dynamic-update-slice_fusion.3
  1.1 0.0 copy-start.4
  1.2 1.1 bitcast_dynamic-update-slice_fusion.2
  2.2 0.0 copy-done.1
  2.2 0.0 copy-start.15
  2.2 0.0 copy-start.16
  2.3 0.0 copy-start.17
  2.3 0.0 copy-start.18
  2.3 0.0 copy-start.19
  2.3 0.0 copy-start.20
  2.3 0.0 copy-start.11
  2.3 0.0 copy-start.12
  2.4 0.0 copy-done.5
  2.4 0.0 copy-start.13
  2.4 0.0 copy-start.14
  2.4 0.0 copy-start.8
  2.4 0.0 copy-start.9
  2.4 0.0 copy-start.10
  2.4 0.1 copy.26
  2.6 0.0 copy-done.6
  2.6 0.1 copy.27
  2.7 0.0 copy-done.7
  2.7 0.0 copy-done.2
  2.8 0.0 copy-done.3
  2.8 0.0 copy-done.4
  2.9 0.0 copy-start
  2.9 0.0 copy-done.15
  2.9 0.0 copy-done.16
  2.9 0.0 copy-done.17
  2.9 0.0 copy-done.18
  2.9 0.0 copy-done.19
  3.0 0.0 copy-done.20
  3.0 0.0 copy-done.11
  3.0 0.0 copy-done.12
  3.0 0.0 copy-done.13
  3.1 0.0 copy-done.14
  3.1 0.0 copy-done.8
  3.1 0.0 copy-done.9
  3.1 0.0 copy-done.10
  3.2 0.7 pad_maximum_fusion.refs_2_
  3.9 0.0 copy-done
  3.9 192.2 %layer.1 = bf16[256,384]{1,0:T(8,128)(2,1)} custom-call(bf16[256,384]{1,0:T(8,128)(2,1)} %refs_0_.1, bf16[4608,128]{1,0:T(8,128)(2,1)} %copy-done, f32[8,3072]{1,0:T(8,128)} %pad_maximum_fusion.refs_2_, bf16[128,128]{1,0:T(8,128)(2,1)} %bitcast.22, f32[1,128]{1,0:T(1,128)} %refs_4_.1), custom_call_target="tpu_custom_call" | custom-call | tf_op jit(solution)/shard_map/layer/pallas_call | solution.py:618
  196.1 1.6 copy.37
  (14 shorter events, 0.2 us)
Async XLA Ops:
  0.0 2.2 %copy-start.1 = (f32[704,128]{1,0:T(8,128)S(1)}, f32[704,128]{1,0:T(8,128)}, u32[]{:S(2)}) copy-start(f32[704,128]{1,0:T(8,128)} %param.31) | copy-start | bytes 1081348
  0.0 2.4 %copy-start.5 = (f32[128,128]{1,0:T(8,128)S(1)}, f32[128,128]{1,0:T(8,128)}, u32[]{:S(2)}) copy-start(f32[128,128]{1,0:T(8,128)} %param.34) | copy-start | bytes 196612
  0.0 2.6 %copy-start.6 = (f32[128,128]{1,0:T(8,128)S(1)}, f32[128,128]{1,0:T(8,128)}, u32[]{:S(2)}) copy-start(f32[128,128]{1,0:T(8,128)} %param.36) | copy-start | bytes 196612
  0.0 2.7 %copy-start.7 = (f32[128,128]{1,0:T(8,128)S(1)}, f32[128,128]{1,0:T(8,128)}, u32[]{:S(2)}) copy-start(f32[128,128]{1,0:T(8,128)} %param.41) | copy-start | bytes 196612
  0.0 2.7 %copy-start.2 = (f32[128,704]{0,1:T(8,128)S(1)}, f32[128,704]{0,1:T(8,128)}, u32[]{:S(2)}) copy-start(f32[128,704]{0,1:T(8,128)} %param.44) | copy-start | bytes 1081348
  0.0 2.7 %copy-start.3 = (f32[128,704]{0,1:T(8,128)S(1)}, f32[128,704]{0,1:T(8,128)}, u32[]{:S(2)}) copy-start(f32[128,704]{0,1:T(8,128)} %param.46) | copy-start | bytes 1081348
  1.1 1.7 copy-start.4
  2.2 0.7 copy-start.15
  2.2 0.7 copy-start.16
  2.3 0.7 copy-start.17
  2.3 0.7 copy-start.18
  2.3 0.7 copy-start.19
  2.3 0.7 copy-start.20
  2.3 0.7 copy-start.11
  2.3 0.7 copy-start.12
  2.4 0.7 copy-start.13
  2.4 0.7 copy-start.14
  2.4 0.7 copy-start.8
  2.4 0.7 copy-start.9
  2.4 0.7 copy-start.10
  2.9 1.0 copy-start

commit v3 on v2

--- a/solution.py
+++ b/solution.py
@@ -25,6 +25,7 @@
     out_ref,
     w,
     scl,
+    scol,
     cols,
     act,
     xn,
@@ -37,6 +38,7 @@
     sb,
     pr,
     cb,
+    rl,
     rr,
     st,
     st_own,
@@ -51,6 +53,7 @@
     precv,
     csend,
     crecv,
+    lrecv,
     gsend,
     grecv,
     tsend,
@@ -81,7 +84,7 @@
         )
 
     third = ff * 15 // 44
-    alone = (2 * third, third, ch, 2 * third, third)
+    alone = (2 * third, third, ch, 2 * third - 32, third - 48)
     total = (2 * ff, ff, 3 * ch, 2 * ff, ff)
     base, first = [], 0
     for n in total:
@@ -256,19 +259,17 @@
     def to_sibling(r, zs):
         return copy(sb.at[r, zs], pr.at[r, zs], psend.at[r], precv.at[r, zs], sibling)
 
-    def to_owner(r, zs):
-        return copy(
-            cb.at[r, zs],
-            rr.at[r, x, zs % 2],
-            csend.at[r],
-            crecv.at[r],
-            at_tp(2 * (zs // 4) + c),
-        )
-
-    def produce(r, j, lhs, rhs):
+    def to_owner(r, zs, slot):
+        device = (right_x, left_x, at_tp(2 * far + c))[slot - 1]
+        return copy(cb.at[r, zs], rr.at[r, slot, zs % 2], csend.at[r], crecv.at[r], device)
+
+    def to_relay(r, zs, side):
+        return copy(cb.at[r, zs], rl.at[r, side], csend.at[r], lrecv.at[r, side], (right_x, left_x)[side])
+
+    def produce(r, pieces, lhs, rhs):
         product = contract_rows(lhs, rhs)
-        for i, zs in enumerate(pair_of(j)):
-            col = jnp.transpose(scl[zs])[:, r : r + 1]
+        for i, zs in enumerate(pieces):
+            col = scol[zs][:, r : r + 1]
             term = product[i * LANES : (i + 1) * LANES] * col
             mine = (zs // 2) % 2 == c
 
@@ -281,31 +282,75 @@
                 sb[r, zs] = term.astype(BF16)
                 to_sibling(r, zs).start()
 
+    def both_cores(r, zs):
+        to_sibling(r, zs).wait_recv()
+        return pbuf[zs] + pr[r, zs].astype(F32)
+
     def combine(r, j):
         for zs in pair_of(j):
 
             @pl.when((zs // 2) % 2 == c)
             def _():
-                to_sibling(r, zs).wait_recv()
-                both = (pbuf[zs] + pr[r, zs].astype(F32)).astype(BF16)
+                both = both_cores(r, zs).astype(BF16)
 
                 @pl.when(zs // 4 == x)
                 def _():
-                    rr[r, x, zs % 2] = both
+                    rr[r, 0, zs % 2] = both
 
                 @pl.when(zs // 4 != x)
                 def _():
                     cb[r, zs] = both
-                    to_owner(r, zs).start()
+
+                for slot, owner in ((1, xr), (2, xl), (3, far)):
+
+                    @pl.when(zs // 4 == owner)
+                    def _():
+                        to_owner(r, zs, slot).start()
+
+    def turn_of(i):
+        away = jnp.where(i < 2, 2, jnp.where(i < 6, 1 + 2 * (i % 2), 0))
+        return away, (x + away) % nx, ((i + 1) // 2) % 2
+
+    def pieces_of(i):
+        _, owner, q = turn_of(i)
+        return 4 * owner + q, 4 * owner + 2 + q
+
+    def combine_turn(r, i):
+        away, owner, q = turn_of(i)
+        zs = 4 * owner + 2 * c + q
+        both = both_cores(r, zs)
+
+        @pl.when(away == 0)
+        def _():
+            rr[r, 0, q] = both.astype(BF16)
+
+        for side in (0, 1):
+
+            @pl.when(jnp.logical_and(away == 2, q == side))
+            def _():
+                cb[r, zs] = both.astype(BF16)
+                to_relay(r, zs, side).start()
+
+            @pl.when(jnp.logical_and(away == 1 + 2 * side, q != side))
+            def _():
+                cb[r, zs] = both.astype(BF16)
+                to_owner(r, zs, 1 + side).start()
+
+            @pl.when(jnp.logical_and(away == 1 + 2 * side, q == side))
+            def _():
+                to_relay(r, zs, side).wait_recv()
+                cb[r, zs] = (both + rl[r, side].astype(F32)).astype(BF16)
+                to_owner(r, zs, 1 + side).start()
 
     def finish(r, factor):
-        arrived = cb.at[r, pl.ds(0, 2 * (nx - 1))]
+        slots = (0, 1, 2, 3) if r == 0 else (0, 1, 2)
+        arrived = cb.at[r, pl.ds(0, 2 * len(slots) - 2)]
         copy(arrived, arrived, csend.at[r], crecv.at[r], sibling).wait_recv()
         news = []
         for h in (0, 1):
             summed = rr[r, 0, h].astype(F32)
-            for xs in range(1, nx):
-                summed = summed + rr[r, xs, h].astype(F32)
+            for slot in slots[1:]:
+                summed = summed + rr[r, slot, h].astype(F32)
             at = pl.ds(pl.multiple_of(t * rows + h * LANES, LANES), LANES)
             news.append((act[r, at].astype(F32) + factor * summed).astype(BF16))
         return news
@@ -320,10 +365,10 @@
         sent = cb.at[r, pl.ds(0, 2 * (nx - 1))]
         copy(sent, sent, csend.at[r], crecv.at[r], sibling).wait_send()
 
-    def down_piece(p, r, j):
-        a, b = pair_of(j)
+    def down_piece(p, r, pieces):
+        a, b = pieces
         lhs = jnp.concatenate([w[a, pl.ds(base[p], ff)], w[b, pl.ds(base[p], ff)]], axis=1)
-        produce(r, j, lhs, hid[...])
+        produce(r, pieces, lhs, hid[...])
 
     fetch_stream = pltpu.make_async_copy(stream_ref, act.at[0, own_rows], in_sem.at[0])
     fetch_scale = pltpu.make_async_copy(
@@ -395,6 +440,15 @@
     scale_tick(half)
     hidden(0)
 
+    def turn_scale(q, _):
+        scol[q] = jnp.transpose(scl[q])
+        return 0
+
+    lax.fori_loop(0, nz, turn_scale, 0)
+
+    def inside(j):
+        return jnp.logical_and(j >= 1, j <= half)
+
     def second_loop(j, _):
         @pl.when(j + 1 <= half)
         def _():
@@ -406,17 +460,18 @@
             start_ring(3)
             start_ring(4)
 
-        wait_across(1, j)
-        down_piece(1, 0, j)
-
-        @pl.when(j > 1)
+        @pl.when(j <= half)
+        def _():
+            wait_across(1, j)
+            down_piece(1, 0, pair_of(j))
+
+        @pl.when(inside(j - 1))
         def _():
             combine(0, j - 1)
 
         return 0
 
-    lax.fori_loop(1, half + 1, second_loop, 0)
-    combine(0, half)
+    lax.fori_loop(1, half + 2, second_loop, 0)
     tick(3, 1)
     next_stream(0, 0.5)
     gather_start(1)
@@ -467,67 +522,75 @@
         )
         gated[:, at] = (left[:, at] * (mixed + bias_ref[...])).astype(BF16)
 
-    def mixer_out_loop(j, _):
-        a, b = pair_of(j)
-        here = pl.ds(base[2] + 2 * ch, ch)
-        produce(1, j, jnp.concatenate([w[a, here], w[b, here]], axis=1), gated[...])
-
-        @pl.when(j > 2)
-        def _():
-            combine(1, j - 2)
-
-        @pl.when(j == half // 2)
+    def mixer_out_loop(i, _):
+        @pl.when(i < half)
+        def _():
+            a, b = pieces_of(i)
+            here = pl.ds(base[2] + 2 * ch, ch)
+            produce(1, (a, b), jnp.concatenate([w[a, here], w[b, here]], axis=1), gated[...])
+
+        @pl.when(i >= 3)
+        def _():
+            combine_turn(1, i - 3)
+
+        @pl.when(i == 3)
         def _():
             tick(3, 4)
 
+        @pl.when(i == half)
+        def _():
+            tick(4, 4)
+
         return 0
 
-    lax.fori_loop(1, half + 1, mixer_out_loop, 0)
-    tick(4, 4)
-    combine(1, half - 1)
-    combine(1, half)
+    lax.fori_loop(0, half + 3, mixer_out_loop, 0)
     tick(3, 5)
     next_stream(1, 1.0)
     gather_start(2)
     tick(4, 5)
+    gather_middle(2)
     tick(3, 6)
-    gather_middle(2)
+    gather_end(2)
     tick(4, 6)
-    gather_end(2)
     normalise(2)
     clear(2 * ff)
+    tick(3, half - 1)
 
     def third_loop(j, _):
-        @pl.when(j == half - 3)
-        def _():
-            tick(3, half - 1)
+        @pl.when(j == 2)
+        def _():
             tick(4, half - 1)
 
+        @pl.when(j == half - 2)
+        def _():
+            tick(3, half)
+
         @pl.when(j == half - 1)
         def _():
-            tick(3, half)
+            tick(4, half)
 
         wait_across(3, j)
         project_pair(base[3], 2 * ff, j, ff // 2)
         return 0
 
     lax.fori_loop(1, half + 1, third_loop, 0)
-    tick(4, half)
     hidden(1)
 
-    def fourth_loop(j, _):
+    for j in range(1, half + 1):
         wait_across(4, j)
-        down_piece(4, 2, j)
-
-        @pl.when(j > 2)
-        def _():
-            combine(2, j - 2)
+
+    def fourth_loop(i, _):
+        @pl.when(i < half)
+        def _():
+            down_piece(4, 2, pieces_of(i))
+
+        @pl.when(i >= 2)
+        def _():
+            combine_turn(2, i - 2)
 
         return 0
 
-    lax.fori_loop(1, half + 1, fourth_loop, 0)
-    combine(2, half - 1)
-    combine(2, half)
+    lax.fori_loop(0, half + 2, fourth_loop, 0)
     for h, new in enumerate(finish(2, 0.5)):
         out_ref[h * LANES : (h + 1) * LANES] = new
 
@@ -623,6 +686,7 @@
             scratch_shapes=[
                 pltpu.VMEM((nz, depth, LANES), BF16),
                 pltpu.VMEM((nz, 8, LANES), F32),
+                pltpu.VMEM((nz, LANES, 8), F32),
                 pltpu.VMEM((vectors.shape[1], 8), F32),
                 pltpu.VMEM((3, whole, toks), BF16),
                 pltpu.VMEM((whole, toks), BF16),
@@ -635,7 +699,8 @@
                 pltpu.VMEM((3, *piece), BF16),
                 pltpu.VMEM((3, *piece), BF16),
                 pltpu.VMEM((3, *piece), BF16),
-                pltpu.VMEM((3, ntp // 2, 2, LANES, toks), BF16),
+                pltpu.VMEM((3, 2, LANES, toks), BF16),
+                pltpu.VMEM((3, 4, 2, LANES, toks), BF16),
                 pltpu.VMEM((ntp, 8, toks), F32),
                 pltpu.VMEM((8, toks), F32),
                 dma((7,)),
@@ -649,6 +714,7 @@
                 dma((3, nz)),
                 dma((3,)),
                 dma((3,)),
+                dma((3, 2)),
                 dma((3,)),
                 dma((3, 7)),
                 dma((1,)),

time: 198 us -> 192 us (0.970)
  Pallas kernels: 192 us -> 186 us
    pallas_call x1, Pallas kernels: 192 us -> 186 us  [local(): pl.pallas_call(body, out_shape=jax.ShapeDtypeStruct((rows, toks), BF16),...]
where the time goes in v3:
time: 192 us
  Pallas kernels  186 us (97%)
  other arithmetic  3.09 us (2%)
  local copies, waits for them, and re-layouts  2.15 us (1%)
    pallas_call x1, Pallas kernels, local(): pl.pallas_call(body, out_shape=jax.ShapeDtypeStruct((rows, toks), BF16),...  186 us

profile of v3, /device:TPU:33, one launch (start us, length us, event | category | flops | bytes accessed | tf_op | source)
XLA Modules:
  0.0 191.8 jit_solution(5628389522064275878)
XLA Ops:
  0.0 0.0 copy-start.1
  0.0 0.0 copy-start.5
  0.0 0.0 copy-start.6
  0.0 0.0 copy-start.7
  0.0 0.0 copy-start.2
  0.0 0.0 copy-start.3
  0.0 1.1 bitcast_dynamic-update-slice_fusion.3
  1.1 0.0 copy-start.4
  1.2 1.1 bitcast_dynamic-update-slice_fusion.2
  2.2 0.0 copy-done.1
  2.2 0.0 copy-start.15
  2.2 0.0 copy-start.16
  2.3 0.0 copy-start.17
  2.3 0.0 copy-start.18
  2.3 0.0 copy-start.19
  2.3 0.0 copy-start.20
  2.3 0.0 copy-start.11
  2.3 0.0 copy-start.12
  2.4 0.0 copy-done.5
  2.4 0.0 copy-start.13
  2.4 0.0 copy-start.14
  2.4 0.0 copy-start.8
  2.4 0.0 copy-start.9
  2.4 0.0 copy-start.10
  2.4 0.1 copy.26
  2.6 0.0 copy-done.6
  2.6 0.1 copy.27
  2.7 0.0 copy-done.7
  2.7 0.0 copy-done.2
  2.8 0.0 copy-done.3
  2.8 0.0 copy-done.4
  2.9 0.0 copy-start
  2.9 0.0 copy-done.15
  2.9 0.0 copy-done.16
  2.9 0.0 copy-done.17
  2.9 0.0 copy-done.18
  2.9 0.0 copy-done.19
  3.0 0.0 copy-done.20
  3.0 0.0 copy-done.11
  3.0 0.0 copy-done.12
  3.0 0.0 copy-done.13
  3.1 0.0 copy-done.14
  3.1 0.0 copy-done.8
  3.1 0.0 copy-done.9
  3.1 0.0 copy-done.10
  3.2 0.7 pad_maximum_fusion.refs_2_
  3.9 0.0 copy-done
  3.9 186.3 %layer.1 = bf16[256,384]{1,0:T(8,128)(2,1)} custom-call(bf16[256,384]{1,0:T(8,128)(2,1)} %refs_0_.1, bf16[4608,128]{1,0:T(8,128)(2,1)} %copy-done, f32[8,3072]{1,0:T(8,128)} %pad_maximum_fusion.refs_2_, bf16[128,128]{1,0:T(8,128)(2,1)} %bitcast.22, f32[1,128]{1,0:T(1,128)} %refs_4_.1), custom_call_target="tpu_custom_call" | custom-call | tf_op jit(solution)/shard_map/layer/pallas_call | solution.py:681
  190.2 1.6 copy.37
  (14 shorter events, 0.2 us)
Async XLA Ops:
  0.0 2.2 %copy-start.1 = (f32[704,128]{1,0:T(8,128)S(1)}, f32[704,128]{1,0:T(8,128)}, u32[]{:S(2)}) copy-start(f32[704,128]{1,0:T(8,128)} %param.31) | copy-start | bytes 1081348
  0.0 2.4 %copy-start.5 = (f32[128,128]{1,0:T(8,128)S(1)}, f32[128,128]{1,0:T(8,128)}, u32[]{:S(2)}) copy-start(f32[128,128]{1,0:T(8,128)} %param.34) | copy-start | bytes 196612
  0.0 2.6 %copy-start.6 = (f32[128,128]{1,0:T(8,128)S(1)}, f32[128,128]{1,0:T(8,128)}, u32[]{:S(2)}) copy-start(f32[128,128]{1,0:T(8,128)} %param.36) | copy-start | bytes 196612
  0.0 2.7 %copy-start.7 = (f32[128,128]{1,0:T(8,128)S(1)}, f32[128,128]{1,0:T(8,128)}, u32[]{:S(2)}) copy-start(f32[128,128]{1,0:T(8,128)} %param.41) | copy-start | bytes 196612
  0.0 2.7 %copy-start.2 = (f32[128,704]{0,1:T(8,128)S(1)}, f32[128,704]{0,1:T(8,128)}, u32[]{:S(2)}) copy-start(f32[128,704]{0,1:T(8,128)} %param.44) | copy-start | bytes 1081348
  0.0 2.7 %copy-start.3 = (f32[128,704]{0,1:T(8,128)S(1)}, f32[128,704]{0,1:T(8,128)}, u32[]{:S(2)}) copy-start(f32[128,704]{0,1:T(8,128)} %param.46) | copy-start | bytes 1081348
  1.1 1.7 copy-start.4
  2.2 0.7 copy-start.15
  2.2 0.7 copy-start.16
  2.3 0.7 copy-start.17
  2.3 0.7 copy-start.18
  2.3 0.7 copy-start.19
  2.3 0.7 copy-start.20
  2.3 0.7 copy-start.11
  2.3 0.7 copy-start.12
  2.4 0.7 copy-start.13
  2.4 0.7 copy-start.14
  2.4 0.7 copy-start.8
  2.4 0.7 copy-start.9
  2.4 0.7 copy-start.10
  2.9 1.0 copy-start

commit v4 on v3

--- a/solution.py
+++ b/solution.py
@@ -18,11 +18,22 @@
 def kernel(
     sizes,
     stream_ref,
-    pack_ref,
+    first_gate_ref,
+    first_up_ref,
+    first_down_ref,
+    left_ref,
+    right_ref,
+    mixer_out_ref,
+    second_gate_ref,
+    second_up_ref,
+    second_down_ref,
     vectors_ref,
     spatial_ref,
     bias_ref,
     out_ref,
+    wide,
+    tall,
+    small,
     w,
     scl,
     scol,
@@ -91,6 +102,8 @@
         base.append(first)
         first += n
 
+    y_slot = (0, 1, 2, 0, 3)
+
     def part(p, sub, zs):
         shared = total[p] - 2 * alone[p]
         if sub == 0:
@@ -104,13 +117,13 @@
         return half if d == sub else half - 1
 
     def hop(p, d, sub, zs, k):
-        return copy(part(p, sub, zs), part(p, sub, zs), zsend.at[p], zrecv.at[p, d, sub, k], around[d])
+        return copy(part(p, sub, zs), part(p, sub, zs), zsend.at[p], zrecv.at[p % 3, d, sub, k], around[d])
 
     def scale_hop(d, zs, k):
         return copy(scl.at[zs], scl.at[zs], ssend.at[0], srecv.at[d, k], around[d])
 
     def across(p, zs, k):
-        return copy(part(p, 0, zs), part(p, 0, zs), ysend.at[p], yrecv.at[p, k - 1], partner)
+        return copy(part(p, 0, zs), part(p, 0, zs), ysend.at[p], yrecv.at[y_slot[p], k - 1], partner)
 
     def start_ring(p):
         for sub in (0, 1):
@@ -157,7 +170,7 @@
             @pl.when((j < half) == (several == 2))
             def _():
                 pieces = w.at[pl.ds(0, several), pl.ds(base[p], alone[p])]
-                copy(pieces, pieces, ysend.at[p], yrecv.at[p, j - 1], partner).wait_recv()
+                copy(pieces, pieces, ysend.at[p], yrecv.at[y_slot[p], j - 1], partner).wait_recv()
 
     own_rows = pl.ds(pl.multiple_of(t * rows, rows), rows)
     hr = rows // 2
@@ -166,10 +179,10 @@
         return act.at[r, pl.ds(pl.multiple_of(tt * rows + h * hr, hr), hr)]
 
     def g_half(r, i, tt, h, device):
-        return copy(chunk(r, tt, h), chunk(r, tt, h), gsend.at[r], grecv.at[r, i if i < 7 else 0], device)
+        return copy(chunk(r, tt, h), chunk(r, tt, h), gsend.at[r], grecv.at[i if i < 7 else 0], device)
 
     def g_whole(r):
-        return copy(act.at[r, own_rows], act.at[r, own_rows], gsend.at[r], grecv.at[r, 0], sibling)
+        return copy(act.at[r, own_rows], act.at[r, own_rows], gsend.at[r], grecv.at[0], sibling)
 
     far = (x + 2) % nx
 
@@ -199,11 +212,11 @@
         g_half(r, 6, 2 * far + c, 1, left_x).wait_recv()
         g_half(r, 12, 2 * far + c, 1, sibling).start()
         arrived = act.at[r, pl.ds(0, 4 * rows)]
-        copy(arrived, arrived, gsend.at[r], grecv.at[r, 0], sibling).wait_recv()
+        copy(arrived, arrived, gsend.at[r], grecv.at[0], sibling).wait_recv()
 
     def gather_drain(r):
         sent = act.at[r, pl.ds(0, 7 * rows)]
-        copy(sent, sent, gsend.at[r], grecv.at[r, 0], sibling).wait_send()
+        copy(sent, sent, gsend.at[r], grecv.at[0], sibling).wait_send()
 
     def normalise(r):
         def squares(i, s):
@@ -257,7 +270,7 @@
         lax.fori_loop(0, ff // 64, one, 0)
 
     def to_sibling(r, zs):
-        return copy(sb.at[r, zs], pr.at[r, zs], psend.at[r], precv.at[r, zs], sibling)
+        return copy(sb.at[r, zs], pr.at[r, zs], psend.at[r], precv.at[zs], sibling)
 
     def to_owner(r, zs, slot):
         device = (right_x, left_x, at_tp(2 * far + c))[slot - 1]
@@ -308,8 +321,8 @@
                         to_owner(r, zs, slot).start()
 
     def turn_of(i):
-        away = jnp.where(i < 2, 2, jnp.where(i < 6, 1 + 2 * (i % 2), 0))
-        return away, (x + away) % nx, ((i + 1) // 2) % 2
+        away = jnp.where(i < 2, 2, jnp.where(i // 2 == 2, 0, 1 + 2 * (i % 2)))
+        return away, (x + away) % nx, jnp.where(i < 6, ((i + 1) // 2) % 2, i % 2)
 
     def pieces_of(i):
         _, owner, q = turn_of(i)
@@ -361,7 +374,7 @@
 
     def reduce_drain(r):
         sent = sb.at[r, pl.ds(0, half)]
-        copy(sent, sent, psend.at[r], precv.at[r, 0], sibling).wait_send()
+        copy(sent, sent, psend.at[r], precv.at[0], sibling).wait_send()
         sent = cb.at[r, pl.ds(0, 2 * (nx - 1))]
         copy(sent, sent, csend.at[r], crecv.at[r], sibling).wait_send()
 
@@ -374,33 +387,54 @@
     fetch_scale = pltpu.make_async_copy(
         vectors_ref.at[:, pl.ds(scale_at, LANES)], scl.at[z], in_sem.at[1]
     )
+    shares = (
+        (first_gate_ref, wide.at[0], base[0], True),
+        (first_up_ref, wide.at[1], base[0] + ff, True),
+        (first_down_ref, tall.at[0], base[1], False),
+        (left_ref, small.at[0], base[2], True),
+        (right_ref, small.at[1], base[2] + ch, True),
+        (mixer_out_ref, small.at[2], base[2] + 2 * ch, False),
+        (second_gate_ref, wide.at[2], base[3], True),
+        (second_up_ref, wide.at[3], base[3] + ff, True),
+        (second_down_ref, tall.at[1], base[4], False),
+    )
     fetches = [
-        pltpu.make_async_copy(
-            pack_ref.at[pl.ds(base[p], total[p])], w.at[z, pl.ds(base[p], total[p])], in_sem.at[2 + p]
-        )
-        for p in range(5)
+        pltpu.make_async_copy(src, held, in_sem.at[2 + i]) for i, (src, held, _, _) in enumerate(shares)
     ]
+
+    def catch(i):
+        fetches[i].wait()
+        _, held, at, turned = shares[i]
+        if not turned:
+            w[z, at : at + held.shape[0]] = held[...].astype(BF16)
+            return
+        for n in range(0, held.shape[1], LANES):
+            wid = min(LANES, held.shape[1] - n)
+            w[z, at + n : at + n + wid] = jnp.transpose(held[:, n : n + wid]).astype(BF16)
+
     fetches[0].start()
+    fetches[1].start()
     fetch_stream.start()
     fetch_scale.start()
-    for p in range(1, 5):
-        fetches[p].start()
+    for fetch in fetches[2:]:
+        fetch.start()
 
     barrier = pltpu.get_barrier_semaphore()
     peers = [*around, partner] + [at_tp((t + d) % ntp) for d in range(1, ntp)]
     for device in peers:
         pl.semaphore_signal(barrier, inc=1, device_id=device, device_id_type=MESH)
+    catch(0)
+    catch(1)
     pl.semaphore_wait(barrier, len(peers))
 
-    fetches[0].wait()
     start_ring(0)
     fetch_stream.wait()
     gather_start(0)
     fetch_scale.wait()
     for d in (0, 1):
         scale_hop(d, z, 0).start()
-    for p in range(1, 5):
-        fetches[p].wait()
+    for i in range(2, 9):
+        catch(i)
     clear(2 * ff)
 
     def turn(i, _):
@@ -551,29 +585,29 @@
     gather_middle(2)
     tick(3, 6)
     gather_end(2)
-    tick(4, 6)
     normalise(2)
     clear(2 * ff)
-    tick(3, half - 1)
 
     def third_loop(j, _):
         @pl.when(j == 2)
         def _():
+            tick(3, half - 1)
+            tick(4, half - 2)
+
+        @pl.when(j == half - 3)
+        def _():
+            tick(3, half)
+
+        @pl.when(j == half - 1)
+        def _():
             tick(4, half - 1)
-
-        @pl.when(j == half - 2)
-        def _():
-            tick(3, half)
-
-        @pl.when(j == half - 1)
-        def _():
-            tick(4, half)
 
         wait_across(3, j)
         project_pair(base[3], 2 * ff, j, ff // 2)
         return 0
 
     lax.fori_loop(1, half + 1, third_loop, 0)
+    tick(4, half)
     hidden(1)
 
     for j in range(1, half + 1):
@@ -596,9 +630,9 @@
 
     for p in range(5):
         sent = w.at[pl.ds(0, nz - 1), pl.ds(base[p], total[p] - alone[p])]
-        copy(sent, sent, zsend.at[p], zrecv.at[p, 0, 0, 0], sibling).wait_send()
+        copy(sent, sent, zsend.at[p], zrecv.at[0, 0, 0, 0], sibling).wait_send()
         sent = w.at[pl.ds(0, nz - 1), pl.ds(base[p], alone[p])]
-        copy(sent, sent, ysend.at[p], yrecv.at[p, 0], sibling).wait_send()
+        copy(sent, sent, ysend.at[p], yrecv.at[0, 0], sibling).wait_send()
     sent = scl.at[pl.ds(0, nz - 1)]
     copy(sent, sent, ssend.at[0], srecv.at[0, 0], sibling).wait_send()
     for r in range(3):
@@ -642,21 +676,6 @@
         width, ff = first_gate.shape
         ch, span = mixer_left.shape[1], spatial.shape[1]
         whole = width * nz
-        pack = jnp.concatenate(
-            [
-                first_gate.T,
-                first_up.T,
-                first_down,
-                mixer_left.T,
-                mixer_right.T,
-                mixer_out,
-                second_gate.T,
-                second_up.T,
-                second_down,
-            ],
-            axis=0,
-        ).astype(BF16)
-
         def eight_rows(*vectors):
             return jnp.pad(jnp.stack(vectors), ((0, 8 - len(vectors)), (0, -vectors[0].shape[0] % LANES)))
 
@@ -669,7 +688,7 @@
             ],
             axis=1,
         )
-        depth = pack.shape[0]
+        depth = 6 * ff + 3 * ch
         dma, half = pltpu.SemaphoreType.DMA, nz // 2
         vmem, anywhere = pl.BlockSpec(memory_space=pltpu.VMEM), pl.BlockSpec(memory_space=pl.ANY)
         sizes = (nz, ntp, ff, ch, span)
@@ -681,9 +700,12 @@
         return pl.pallas_call(
             body,
             out_shape=jax.ShapeDtypeStruct((rows, toks), BF16),
-            in_specs=[anywhere, anywhere] + [vmem] * 3,
+            in_specs=[anywhere] * 10 + [vmem] * 3,
             out_specs=vmem,
             scratch_shapes=[
+                pltpu.VMEM((4, width, ff), F32),
+                pltpu.VMEM((2, ff, width), F32),
+                pltpu.VMEM((3, width, ch), F32),
                 pltpu.VMEM((nz, depth, LANES), BF16),
                 pltpu.VMEM((nz, 8, LANES), F32),
                 pltpu.VMEM((nz, LANES, 8), F32),
@@ -703,20 +725,20 @@
                 pltpu.VMEM((3, 4, 2, LANES, toks), BF16),
                 pltpu.VMEM((ntp, 8, toks), F32),
                 pltpu.VMEM((8, toks), F32),
-                dma((7,)),
+                dma((11,)),
                 dma((5,)),
-                dma((5, 2, 2, half)),
+                dma((3, 2, 2, half)),
                 dma((1,)),
                 dma((2, half)),
                 dma((5,)),
-                dma((5, half)),
+                dma((4, half)),
                 dma((3,)),
-                dma((3, nz)),
+                dma((nz,)),
                 dma((3,)),
                 dma((3,)),
                 dma((3, 2)),
                 dma((3,)),
-                dma((3, 7)),
+                dma((7,)),
                 dma((1,)),
                 dma((1,)),
             ],
@@ -724,7 +746,21 @@
                 collective_id=0, has_side_effects=True, vmem_limit_bytes=60 * 1024 * 1024
             ),
             name="layer",
-        )(stream, pack, vectors, spatial.reshape(span, span), spatial_bias)
+        )(
+            stream,
+            first_gate,
+            first_up,
+            first_down,
+            mixer_left,
+            mixer_right,
+            mixer_out,
+            second_gate,
+            second_up,
+            second_down,
+            vectors,
+            spatial.reshape(span, span),
+            spatial_bias,
+        )
 
     return jax.shard_map(
         local,

time: 192 us -> 198 us (1.031)
  local copies, waits for them, and re-layouts: 2.15 us -> 8.31 us
    unnamed x47 -> x13, local copies, waits for them, and re-layouts: 2.13 us -> 5.51 us
    another operation x4, local copies, waits for them, and re-layouts: 0.01 us -> 2.8 us  [eight_rows(): jnp.stack(vectors)]
    unnamed x6 -> x0, other arithmetic: 2.27 us -> none
where the time goes in v4:
time: 198 us
  Pallas kernels  187 us (94%)
  local copies, waits for them, and re-layouts  8.31 us (4%)
  other arithmetic  2.18 us (1%)
    pallas_call x1, Pallas kernels, local(): pl.pallas_call(body, out_shape=jax.ShapeDtypeStruct((rows, toks), BF16),...  187 us
    unnamed x13, local copies, waits for them, and re-layouts  5.51 us

profile of v4, /device:TPU:33, one launch (start us, length us, event | category | flops | bytes accessed | tf_op | source)
XLA Modules:
  0.0 197.7 jit_solution(12931108989333820912)
XLA Ops:
  0.0 0.0 copy-start
  0.0 0.7 stack.55
  0.7 0.7 stack.56
  1.4 0.7 stack.57
  2.1 0.7 stack.58
  2.8 0.7 select_maximum_fusion.5
  3.6 0.8 select_maximum_fusion
  4.3 0.6 pad_maximum_fusion.refs_10_
  5.0 0.0 copy-done
  5.0 0.0 copy-start.1
  5.0 0.9 copy.26.refs_1_
  5.9 0.1 copy-done.1
  6.0 0.0 copy-start.2
  6.0 0.9 copy.27.refs_2_
  6.9 0.1 copy-done.2
  7.0 0.0 copy-start.3
  7.0 0.9 copy.28.refs_7_
  7.9 0.1 copy-done.3
  8.0 0.9 copy.29.refs_8_
  8.9 187.2 %layer.1 = bf16[256,384]{1,0:T(8,128)(2,1)} custom-call(bf16[256,384]{1,0:T(8,128)(2,1)} %refs_0_.1, f32[128,704]{1,0:T(8,128)} %copy.26.refs_1_, f32[128,704]{1,0:T(8,128)} %copy.27.refs_2_, f32[704,128]{1,0:T(8,128)} %refs_3_.1, f32[128,128]{1,0:T(8,128)} %refs_4_.1, f32[128,128]{1,0:T(8,128)} %refs_5_.1, f32[128,128]{1,0:T(8,128)} %refs_6_.1, ...), custom_call_target="tpu_custom_call" | custom-call | tf_op jit(solution)/shard_map/layer/pallas_call | solution.py:700
  196.0 1.6 copy.31
  (1 shorter events, 0.0 us)
Async XLA Ops:
  0.0 5.0 %copy-start = (f32[128,704]{0,1:T(8,128)S(1)}, f32[128,704]{0,1:T(8,128)}, u32[]{:S(2)}) copy-start(f32[128,704]{0,1:T(8,128)} %param.27) | copy-start | bytes 1081348
  5.0 1.0 copy-start.1
  6.0 1.0 copy-start.2
  7.0 1.0 copy-start.3

commit v5 on v4

--- a/solution.py
+++ b/solution.py
@@ -27,13 +27,37 @@
     second_gate_ref,
     second_up_ref,
     second_down_ref,
-    vectors_ref,
     spatial_ref,
     bias_ref,
+    *rest,
+):
+    vector_refs, rest = rest[:13], rest[13:]
+    layer(
+        sizes,
+        (stream_ref, vector_refs, spatial_ref, bias_ref),
+        (
+            first_gate_ref,
+            first_up_ref,
+            first_down_ref,
+            left_ref,
+            right_ref,
+            mixer_out_ref,
+            second_gate_ref,
+            second_up_ref,
+            second_down_ref,
+        ),
+        *rest,
+    )
+
+
+def layer(
+    sizes,
+    inputs,
+    weights,
     out_ref,
-    wide,
     tall,
     small,
+    vectors_ref,
     w,
     scl,
     scol,
@@ -71,6 +95,7 @@
     trecv,
 ):
     nz, ntp, ff, ch, span = sizes
+    stream_ref, vector_refs, spatial_ref, bias_ref = inputs
     nx, half = ntp // 2, nz // 2
     hidden_at = vectors_ref.shape[1] - 2 * LANES - (-ff % LANES) - ff
     mixer_at = vectors_ref.shape[1] - 2 * LANES
@@ -384,19 +409,17 @@
         produce(r, pieces, lhs, hid[...])
 
     fetch_stream = pltpu.make_async_copy(stream_ref, act.at[0, own_rows], in_sem.at[0])
-    fetch_scale = pltpu.make_async_copy(
-        vectors_ref.at[:, pl.ds(scale_at, LANES)], scl.at[z], in_sem.at[1]
-    )
+    first_gate, first_up, first_down, left_w, right_w, mixer_out, second_gate, second_up, second_down = weights
     shares = (
-        (first_gate_ref, wide.at[0], base[0], True),
-        (first_up_ref, wide.at[1], base[0] + ff, True),
-        (first_down_ref, tall.at[0], base[1], False),
-        (left_ref, small.at[0], base[2], True),
-        (right_ref, small.at[1], base[2] + ch, True),
-        (mixer_out_ref, small.at[2], base[2] + 2 * ch, False),
-        (second_gate_ref, wide.at[2], base[3], True),
-        (second_up_ref, wide.at[3], base[3] + ff, True),
-        (second_down_ref, tall.at[1], base[4], False),
+        (first_gate, tall.at[0], base[0], False),
+        (first_up, tall.at[1], base[0] + ff, False),
+        (first_down, tall.at[2], base[1], False),
+        (left_w, small.at[0], base[2], True),
+        (right_w, small.at[1], base[2] + ch, True),
+        (mixer_out, small.at[2], base[2] + 2 * ch, False),
+        (second_gate, tall.at[3], base[3], False),
+        (second_up, tall.at[4], base[3] + ff, False),
+        (second_down, tall.at[5], base[4], False),
     )
     fetches = [
         pltpu.make_async_copy(src, held, in_sem.at[2 + i]) for i, (src, held, _, _) in enumerate(shares)
@@ -415,7 +438,6 @@
     fetches[0].start()
     fetches[1].start()
     fetch_stream.start()
-    fetch_scale.start()
     for fetch in fetches[2:]:
         fetch.start()
 
@@ -423,6 +445,12 @@
     peers = [*around, partner] + [at_tp((t + d) % ntp) for d in range(1, ntp)]
     for device in peers:
         pl.semaphore_signal(barrier, inc=1, device_id=device, device_id_type=MESH)
+    vectors_ref[...] = jnp.zeros_like(vectors_ref)
+    places = [(i, 0) for i in range(3)] + [(i, hidden_at) for i in range(4)]
+    places += [(i, mixer_at) for i in range(3)] + [(i, scale_at) for i in range(3)]
+    for ref, (row, at) in zip(vector_refs, places):
+        vectors_ref[row : row + 1, at : at + ref.shape[1]] = ref[...]
+    scl[z] = vectors_ref[:, scale_at : scale_at + LANES]
     catch(0)
     catch(1)
     pl.semaphore_wait(barrier, len(peers))
@@ -430,7 +458,6 @@
     start_ring(0)
     fetch_stream.wait()
     gather_start(0)
-    fetch_scale.wait()
     for d in (0, 1):
         scale_hop(d, z, 0).start()
     for i in range(2, 9):
@@ -676,18 +703,25 @@
         width, ff = first_gate.shape
         ch, span = mixer_left.shape[1], spatial.shape[1]
         whole = width * nz
-        def eight_rows(*vectors):
-            return jnp.pad(jnp.stack(vectors), ((0, 8 - len(vectors)), (0, -vectors[0].shape[0] % LANES)))
-
-        vectors = jnp.concatenate(
-            [
-                eight_rows(first_gain, mixer_gain, second_gain),
-                eight_rows(first_gate_scale, first_up_scale, second_gate_scale, second_up_scale),
-                eight_rows(mixer_left_scale, mixer_right_scale, channel_gain),
-                eight_rows(first_down_scale, mixer_out_scale, second_down_scale),
-            ],
-            axis=1,
-        )
+        vectors = [
+            v.reshape(1, -1)
+            for v in (
+                first_gain,
+                mixer_gain,
+                second_gain,
+                first_gate_scale,
+                first_up_scale,
+                second_gate_scale,
+                second_up_scale,
+                mixer_left_scale,
+                mixer_right_scale,
+                channel_gain,
+                first_down_scale,
+                mixer_out_scale,
+                second_down_scale,
+            )
+        ]
+        lanes = whole + ff + -ff % LANES + 2 * LANES
         depth = 6 * ff + 3 * ch
         dma, half = pltpu.SemaphoreType.DMA, nz // 2
         vmem, anywhere = pl.BlockSpec(memory_space=pltpu.VMEM), pl.BlockSpec(memory_space=pl.ANY)
@@ -700,16 +734,16 @@
         return pl.pallas_call(
             body,
             out_shape=jax.ShapeDtypeStruct((rows, toks), BF16),
-            in_specs=[anywhere] * 10 + [vmem] * 3,
+            in_specs=[anywhere] * 10 + [vmem] * 15,
             out_specs=vmem,
             scratch_shapes=[
-                pltpu.VMEM((4, width, ff), F32),
-                pltpu.VMEM((2, ff, width), F32),
+                pltpu.VMEM((6, ff, width), F32),
                 pltpu.VMEM((3, width, ch), F32),
+                pltpu.VMEM((8, lanes), F32),
                 pltpu.VMEM((nz, depth, LANES), BF16),
                 pltpu.VMEM((nz, 8, LANES), F32),
                 pltpu.VMEM((nz, LANES, 8), F32),
-                pltpu.VMEM((vectors.shape[1], 8), F32),
+                pltpu.VMEM((lanes, 8), F32),
                 pltpu.VMEM((3, whole, toks), BF16),
                 pltpu.VMEM((whole, toks), BF16),
                 pltpu.VMEM((2 * ff, toks), F32),
@@ -748,18 +782,18 @@
             name="layer",
         )(
             stream,
-            first_gate,
-            first_up,
+            first_gate.T,
+            first_up.T,
             first_down,
             mixer_left,
             mixer_right,
             mixer_out,
-            second_gate,
-            second_up,
+            second_gate.T,
+            second_up.T,
             second_down,
-            vectors,
             spatial.reshape(span, span),
             spatial_bias,
+            *vectors,
         )
 
     return jax.shard_map(

time: 198 us -> 192 us (0.970)
  local copies, waits for them, and re-layouts: 8.31 us -> 4.86 us
  other arithmetic: 2.18 us -> 0 us
    unnamed x13 -> x9, local copies, waits for them, and re-layouts: 5.51 us -> 2.53 us
    another operation x4 -> x0, local copies, waits for them, and re-layouts: 2.8 us -> none  [eight_rows(): jnp.stack(vectors)]
    reshape x0 -> x4, local copies, waits for them, and re-layouts: none -> 2.34 us  [local(): v.reshape(1, -1)]
where the time goes in v5:
time: 192 us
  Pallas kernels  187 us (97%)
  local copies, waits for them, and re-layouts  4.86 us (3%)
    pallas_call x1, Pallas kernels, local(): pl.pallas_call(body, out_shape=jax.ShapeDtypeStruct((rows, toks), BF16),...  187 us

profile of v5, /device:TPU:33, one launch (start us, length us, event | category | flops | bytes accessed | tf_op | source)
XLA Modules:
  0.0 192.0 jit_solution(5939658949343335576)
XLA Ops:
  0.0 0.0 copy-start
  0.0 0.0 copy-start.1
  0.0 0.7 copy-done
  0.7 0.6 reshape.46.refs_15_
  1.3 0.0 copy-done.1
  1.3 0.0 copy-start.2
  1.3 0.6 reshape.47.refs_16_
  1.9 0.1 copy-done.2
  2.0 0.0 copy-start.3
  2.0 0.6 reshape.48.refs_17_
  2.5 0.1 copy-done.3
  2.7 0.6 reshape.49.refs_18_
  3.2 187.1 %layer.1 = bf16[256,384]{1,0:T(8,128)(2,1)} custom-call(bf16[256,384]{1,0:T(8,128)(2,1)} %refs_0_.1, f32[704,128]{1,0:T(8,128)} %bitcast.14, f32[704,128]{1,0:T(8,128)} %bitcast.15, f32[704,128]{1,0:T(8,128)} %refs_3_.1, f32[128,128]{1,0:T(8,128)} %refs_4_.1, f32[128,128]{1,0:T(8,128)} %refs_5_.1, f32[128,128]{1,0:T(8,128)} %refs_6_.1, f32[704,128]{1,0:T(8,128)} %bitcast.16, ...), custom_call_target="tpu_custom_call" | custom-call | tf_op jit(solution)/shard_map/layer/pallas_call | solution.py:734
  190.4 1.6 copy.27
Async XLA Ops:
  0.0 0.7 copy-start
  0.0 1.3 copy-start.1
  1.3 0.7 copy-start.2
  2.0 0.7 copy-start.3

commit v6 on v5

--- a/solution.py
+++ b/solution.py
@@ -449,7 +449,7 @@
     places = [(i, 0) for i in range(3)] + [(i, hidden_at) for i in range(4)]
     places += [(i, mixer_at) for i in range(3)] + [(i, scale_at) for i in range(3)]
     for ref, (row, at) in zip(vector_refs, places):
-        vectors_ref[row : row + 1, at : at + ref.shape[1]] = ref[...]
+        vectors_ref[row, at : at + ref.shape[0]] = ref[...]
     scl[z] = vectors_ref[:, scale_at : scale_at + LANES]
     catch(0)
     catch(1)
@@ -704,7 +704,7 @@
         ch, span = mixer_left.shape[1], spatial.shape[1]
         whole = width * nz
         vectors = [
-            v.reshape(1, -1)
+            v
             for v in (
                 first_gain,
                 mixer_gain,

time: 192 us -> 189 us (0.984)
  local copies, waits for them, and re-layouts: 4.86 us -> 1.62 us
    reshape x4 -> x0, local copies, waits for them, and re-layouts: 2.34 us -> none  [local(): v.reshape(1, -1)]
where the time goes in v6:
time: 189 us
  Pallas kernels  187 us (99%)
    pallas_call x1, Pallas kernels, local(): pl.pallas_call(body, out_shape=jax.ShapeDtypeStruct((rows, toks), BF16),...  187 us

profile of v6, /device:TPU:33, one launch (start us, length us, event | category | flops | bytes accessed | tf_op | source)
XLA Modules:
  0.0 188.8 jit_solution(16386347180446366121)
XLA Ops:
  0.0 187.1 %layer.1 = bf16[256,384]{1,0:T(8,128)(2,1)} custom-call(bf16[256,384]{1,0:T(8,128)(2,1)} %refs_0_.1, f32[704,128]{1,0:T(8,128)} %bitcast.5, f32[704,128]{1,0:T(8,128)} %bitcast.6, f32[704,128]{1,0:T(8,128)} %refs_3_.1, f32[128,128]{1,0:T(8,128)} %refs_4_.1, f32[128,128]{1,0:T(8,128)} %refs_5_.1, f32[128,128]{1,0:T(8,128)} %refs_6_.1, f32[704,128]{1,0:T(8,128)} %bitcast.7, ...), custom_call_target="tpu_custom_call" | custom-call | tf_op jit(solution)/shard_map/layer/pallas_call | solution.py:734
  187.2 1.6 copy.27
